TPU v7x, 256 devices: a whole 4x4x8 slice. The times are simulated.
256 devices in a mesh: ep: 16 (over y, x), tp: 16 (over z, core).
Axes of the slice: x: 4, y: 4, z: 8, core: 2. Of those that a mesh axis runs over, the one named last changes fastest.
Arguments:
- queries: bfloat16 [8192, 16, 128], P('ep', 'tp'), may hold values from -300 to 300
- keys: bfloat16 [8192, 16, 128], P('ep', 'tp'), may hold values from -4 to 4
- values: bfloat16 [8192, 16, 128], P('ep', 'tp'), may hold values from -6 to 6
- mix_weight: float32 [16], P('tp'), may hold values from 0.3 to 0.8
- sub_gain: float32 [128], replicated, may hold values from 0.1 to 1.9
- tokens: bfloat16 [4096, 2048], P('ep', 'tp'), may hold values from -6 to 6
- routes: int32 [4096, 2], P('ep'), may hold values from 0 to 31, all different within a row; in each aligned block of 256 rows (0 to 255, 256 to 511, ...) at most 24 rows name the same one
- route_weights: float32 [4096, 2], P('ep'), may hold values from 0.1 to 1
- expert_gain: float32 [2048], replicated, may hold values from 0.1 to 1.9
- gate_weight: bfloat16 [32, 2048, 4096], P('ep', None, 'tp'), may hold values from -0.375 to 0.375
- up_weight: bfloat16 [32, 2048, 4096], P('ep', None, 'tp'), may hold values from -0.375 to 0.375
- down_weight: bfloat16 [32, 4096, 2048], P('ep', 'tp'), may hold values from -0.09375 to 0.09375
Outputs:
- attn_out: bfloat16 [8192, 16, 128], P('ep', 'tp')
- moe_out: bfloat16 [4096, 2048], P('ep', 'tp')
Inputs may be any that keep to these rules, and one draw needn't show every extreme that they name: `routes`: in each aligned block of 256 rows no expert is named by more than 24 rows, and in every draw some expert is named by exactly 24 rows of some block.
All inputs are finite; a program needn't handle non-finite values.
Results may differ from a plain program's by a relative error of at most 0.018.
Values may be sent and summed in bfloat16 or wider, within the bound.
A program may use at most 128 MiB of HBM per device.

v0:
```python
import math

import jax
import jax.numpy as jnp
from jax import lax
from jax.sharding import PartitionSpec as P

NEG_FILL = -1e30
SUB_EPS = 1e-05
NORM_EPS = 1e-06
CLAMP_LIMIT = 7.0
GLU_ALPHA = 1.702
OUT_SCALE = 0.8


def side_by_side(arrays, axis, dim, along):
    ends, at = ([], 0)
    for a in arrays[:-1]:
        at += a.shape[along]
        ends.append(at)
    both = jnp.concatenate(arrays, axis=along)
    return tuple(jnp.split(lax.all_gather(both, axis, axis=dim, tiled=True), ends, axis=along))


def split_up(value, dim, count):
    before, after = (value.shape[:dim], value.shape[dim + 1 :])
    return jnp.moveaxis(value.reshape(*before, count, -1, *after), dim, 0)


def sum_at_owner(value, axis, dim):
    count = lax.axis_size(axis)
    tiles = lax.all_to_all(split_up(value, dim, count), axis, 0, 0, tiled=True)
    return jnp.sum(tiles.astype(jnp.float32), axis=0)


def score_update(running, query_four, key_block, value_block, key_start, query_pos, score_scale):
    row_max, row_sum, weighted = running
    item_count = key_block.shape[0]
    key_four = key_block.reshape(item_count, key_block.shape[1], 2, -1)
    scores = (
        jnp.einsum("qhmd,khmd->hmqk", query_four, key_four, preferred_element_type=jnp.float32)
        * score_scale
    )
    key_pos = key_start + lax.iota(jnp.int32, item_count)
    visible = key_pos[None, :] <= query_pos[:, None]
    new_max = jnp.maximum(row_max, jnp.max(jnp.where(visible, scores, NEG_FILL), axis=-1))
    weights = jnp.where(visible, jnp.exp(scores - new_max[..., None]), 0.0)
    shrink = jnp.exp(row_max - new_max)
    row_sum = row_sum * shrink + jnp.sum(weights, axis=-1)
    value_sum = jnp.einsum(
        "hmqk,khe->hmqe",
        weights.astype(jnp.bfloat16),
        value_block,
        preferred_element_type=jnp.float32,
    )
    return (new_max, row_sum, weighted * shrink[..., None] + value_sum)


def attend(queries, keys, values, mix_weight, sub_gain):
    row_count, heads_here, pair_width = queries.shape
    value_width = values.shape[2]
    place = lax.axis_index("ep")
    query_pos = place * row_count + lax.iota(jnp.int32, row_count)
    query_four = queries.reshape(row_count, heads_here, 2, pair_width // 2)
    score_scale = (pair_width // 2) ** (-0.5)
    last_pos = jnp.max(query_pos)
    initial = (
        jnp.full((heads_here, 2, row_count), NEG_FILL, jnp.float32),
        jnp.zeros((heads_here, 2, row_count), jnp.float32),
        jnp.zeros((heads_here, 2, row_count, value_width), jnp.float32),
    )
    key_piece, value_piece = side_by_side((keys, values), "ep", 0, 1)
    item_count = key_piece.shape[0]
    block_size = math.gcd(item_count, 1536)
    key_blocks = key_piece.reshape(item_count // block_size, block_size, heads_here, pair_width)
    value_blocks = value_piece.reshape(
        item_count // block_size, block_size, heads_here, value_width
    )

    def key_step(current, bundle):
        key_block, value_block, block_index = bundle
        key_start = block_index * block_size

        def update(inner):
            return score_update(
                inner, query_four, key_block, value_block, key_start, query_pos, score_scale
            )

        def keep_state(inner):
            return inner

        return (lax.cond(key_start <= last_pos, update, keep_state, current), None)

    result, _ = lax.scan(
        key_step, initial, (key_blocks, value_blocks, lax.iota(jnp.int32, item_count // block_size))
    )
    row_max, row_sum, weighted = result
    heads_out = weighted / row_sum[..., None]
    blend = heads_out[:, 0] - mix_weight[:, None, None] * heads_out[:, 1]
    scaled = blend * lax.rsqrt(jnp.mean(blend * blend, axis=-1, keepdims=True) + SUB_EPS)
    result = jnp.transpose((scaled * sub_gain * OUT_SCALE).astype(jnp.bfloat16), (1, 0, 2))
    return result


def slot_table(routes, experts_all, capacity):
    flat_routes = routes.reshape(-1)
    onehot = (flat_routes[:, None] == lax.iota(jnp.int32, experts_all)[None, :]).astype(jnp.int32)
    slot_rank = jnp.sum((jnp.cumsum(onehot, axis=0) - 1) * onehot, axis=1)
    return flat_routes * capacity + slot_rank


def dispatch(rows_here, target, pick_count, slot_count):
    row_count = rows_here.shape[0]
    slot_owner = (
        jnp.full((slot_count,), row_count, jnp.int32)
        .at[target]
        .set(lax.iota(jnp.int32, row_count * pick_count) // pick_count)
    )
    padded = jnp.concatenate(
        [rows_here, jnp.zeros((1, rows_here.shape[1]), rows_here.dtype)], axis=0
    )
    return padded[slot_owner]


def expert_finish(gate_pre, up_pre, squares, width_total, down_weight):
    factor = lax.rsqrt(squares / width_total + NORM_EPS)[..., None]
    gate_part = jnp.minimum(gate_pre * factor, CLAMP_LIMIT)
    up_part = jnp.clip(up_pre * factor, -CLAMP_LIMIT, CLAMP_LIMIT)
    hidden = ((up_part + 1.0) * gate_part * jax.nn.sigmoid(GLU_ALPHA * gate_part)).astype(
        jnp.bfloat16
    )
    return jnp.einsum("secf,efd->secd", hidden, down_weight, preferred_element_type=jnp.float32)


def route_layer(tokens, routes, route_weights, expert_gain, gate_weight, up_weight, down_weight):
    row_count, pick_count = routes.shape
    groups = lax.axis_size("ep")
    local_experts = gate_weight.shape[0]
    experts_all = groups * local_experts
    capacity = 3 * row_count * pick_count // (2 * experts_all)
    target = slot_table(routes, experts_all, capacity)
    layout = (groups, local_experts, capacity)
    width_total = expert_gain.shape[0]
    outgoing = dispatch(tokens, target, pick_count, experts_all * capacity).reshape(
        layout + (tokens.shape[1],)
    )
    arrived = lax.all_to_all(outgoing, "ep", split_axis=0, concat_axis=0, tiled=True)
    floats = lax.all_gather(arrived, "tp", axis=3, tiled=True).astype(jnp.float32)
    normed = (floats * expert_gain).astype(jnp.bfloat16)
    gate_acc = jnp.einsum("secd,edf->secf", normed, gate_weight, preferred_element_type=jnp.float32)
    up_acc = jnp.einsum("secd,edf->secf", normed, up_weight, preferred_element_type=jnp.float32)
    squares = jnp.sum(floats * floats, axis=-1)
    partial_value = expert_finish(gate_acc, up_acc, squares, width_total, down_weight)
    summed = sum_at_owner(partial_value.astype(jnp.bfloat16), "tp", 3).astype(jnp.bfloat16)
    returned = lax.all_to_all(summed, "ep", split_axis=0, concat_axis=0, tiled=True)
    flat_back = returned.reshape(experts_all * capacity, returned.shape[3])
    picked = flat_back[target].astype(jnp.float32).reshape(row_count, pick_count, returned.shape[3])
    return jnp.sum(picked * route_weights[..., None], axis=1).astype(jnp.bfloat16)


def shards(
    queries,
    keys,
    values,
    mix_weight,
    sub_gain,
    tokens,
    routes,
    route_weights,
    expert_gain,
    gate_weight,
    up_weight,
    down_weight,
):
    attn_out = attend(queries, keys, values, mix_weight, sub_gain)
    moe_out = route_layer(
        tokens, routes, route_weights, expert_gain, gate_weight, up_weight, down_weight
    )
    return (attn_out, moe_out)


def solution(mesh):
    return jax.shard_map(
        shards,
        mesh=mesh,
        in_specs=(
            P("ep", "tp", None),
            P("ep", "tp", None),
            P("ep", "tp", None),
            P("tp"),
            P(),
            P("ep", "tp"),
            P("ep", None),
            P("ep", None),
            P(),
            P("ep", None, "tp"),
            P("ep", None, "tp"),
            P("ep", "tp", None),
        ),
        out_specs=(P("ep", "tp", None), P("ep", "tp")),
        check_vma=False,
    )
```

profile of v0, /device:TPU:1, one launch (start us, length us, event | category | flops | bytes accessed | tf_op | source)
XLA Modules:
  0.0 263.4 jit_solution(11813084081454908823)
XLA Ops:
  7.2 0.0 copy-start
  7.2 0.0 all-gather.5.cloned.1.call-start
  7.2 1.0 copy.62
  8.2 0.1 eq.29
  8.4 0.1 eq.25
  8.5 0.7 broadcast_multiply_fusion
  9.2 1.2 reduce-window.6
  10.4 0.2 slice_reduce_fusion
  10.6 0.1 copy.61
  10.8 0.1 mul.203
  10.9 0.1 fusion.103
  11.1 2.4 scatter_custom_fusion
  13.5 0.8 concatenate.7
  14.4 1.9 gather_fusion
  16.3 14.7 %all_to_all.15 = bf16[16,2,24,128]{3,2,1,0:T(8,128)(2,1)} all-to-all(bf16[16,2,24,128]{3,2,1,0:T(8,128)(2,1)S(1)} %bitcast.156), channel_id=1, replica_groups=mesh['ep'=16,'tp'=16] {'ep'}, dimensions={0} | all-to-all | bytes 393216 | tf_op jit(solution)/shard_map/all_to_all | solution.py:147
  30.9 0.0 all-gather.5.cloned.1.call-update
  31.0 0.0 all-gather.3.cloned.1.call-start
  31.0 0.7 pad_maximum_fusion
  31.8 0.0 all-gather.3.cloned.1.call-update
  31.8 44.7 %all-gather.5.cloned.1.call-done = bf16[16,2,24,2048]{3,2,1,0:T(8,128)(2,1)} async-done(((bf16[16,2,24,128]{3,2,1,0:T(8,128)(2,1)}), bf16[16,2,24,2048]{3,2,1,0:T(8,128)(2,1)}) %all-gather.5.cloned.1.call-update) | async-done | bytes 3145744 | tf_op jit(solution)/shard_map/all_gather | solution.py:148
  76.5 3.0 %fusion.22 = (f32[16,2,24]{2,1,0:T(2,128)S(1)}, bf16[16,2,24,2048]{3,2,1,0:T(8,128)(2,1)S(1)}) fusion(bf16[16,2,24,2048]{3,2,1,0:T(8,128)(2,1)} %all-gather.5.cloned.1.call-done, f32[2048]{0:T(1024)S(1)} %copy-done.5), kind=kLoop, calls=%fused_computation.35 | loop fusion | flops 7863552 | bytes 6302720 | tf_op jit(solution)/shard_map/reduce_sum | solution.py:152
  79.6 1.7 copy-done.1
  81.2 1.1 fusion.48
  82.3 6.3 %fusion.30 = bf16[2,16,3,16,8,128]{5,4,3,2,1,0:T(8,128)(2,1)} fusion(bf16[2,256,2048]{2,1,0:T(8,128)(2,1)S(1)} %copy-done, f32[16,2,24,256]{3,2,0,1:T(8,128)S(1)} %fusion.48, bf16[2,2048,256]{2,1,0:T(8,128)(2,1)} %param.26, bf16[16,2,24,2048]{3,2,1,0:T(8,128)(2,1)} %copy-done.1, f32[16,2,24]{2,0,1:T(8,128)S(1)} %fusion.106), kind=kOutput, calls=%fused_computation.45 | convolution fusion | flops 1614151680 | bytes 11275264 | tf_op jit(solution)/shard_map/secf,efd->secd/dot_general | solution.py:132
  88.6 4.5 %copy.112 = bf16[2,16,3,16,8,128]{5,4,2,1,0,3:T(8,128)(2,1)} copy(bf16[2,16,3,16,8,128]{5,4,3,2,1,0:T(8,128)(2,1)} %fusion.30) | data formatting | bytes 6291456 | tf_op jit(solution)/shard_map/reshape | solution.py:27
  93.1 5.3 %all-to-all-start.1 = ((bf16[16,16,2,24,128]{4,3,1,2,0:T(8,128)(2,1)}), bf16[16,16,2,24,128]{4,3,1,2,0:T(8,128)(2,1)}, u32[]{:S(2)}, u32[]{:S(2)}) async-start(bf16[16,16,2,24,128]{4,3,1,2,0:T(8,128)(2,1)} %bitcast.149), calls=%async_computation.1 | async-start | bytes 6291456 | tf_op jit(solution)/shard_map/all_to_all | solution.py:32
  98.4 0.1 copy.71
  98.5 0.7 add_reduce_fusion
  99.3 0.1 copy.58
  100.0 34.0 %all-gather.3.cloned.1.call-done = bf16[8192,2,128]{2,0,1:T(8,128)(2,1)} async-done(((bf16[512,2,128]{2,0,1:T(8,128)(2,1)}), bf16[8192,2,128]{2,0,1:T(8,128)(2,1)}) %all-gather.3.cloned.1.call-update) | async-done | bytes 4194320 | tf_op jit(solution)/shard_map/all_gather | solution.py:22
  134.1 4.6 %fusion.116 = (bf16[8192,1,128]{2,0,1:T(8,128)(2,1)}, bf16[8192,1,128]{2,0,1:T(8,128)(2,1)}) fusion(bf16[8192,2,128]{2,0,1:T(8,128)(2,1)} %all-gather.3.cloned.1.call-done), kind=kLoop, calls=%fused_computation.108 | loop fusion | bytes 8388608 | tf_op jit(solution)/shard_map/split | solution.py:22
  138.6 3.9 %copy.59 = bf16[16,512,1,128]{1,3,2,0:T(8,128)(2,1)} copy(bf16[16,512,1,128]{3,1,0,2:T(8,128)(2,1)} %bitcast.150) | data formatting | bytes 4194304
  142.6 35.6 %while.15 = (s32[]{:T(128)}, f32[1,2,512]{2,1,0:T(2,128)S(1)}, f32[1,2,512]{2,1,0:T(2,128)S(1)}, f32[1,2,512,128]{3,2,1,0:T(8,128)S(1)}, s32[16]{0:T(128)S(1)}, ...) while((s32[]{:T(128)}, f32[1,2,512]{2,1,0:T(2,128)S(1)}, ...), condition=%wide.region_6.7_spmd.clone, body=%wide.region_1.6_spmd.clone.sunk | while | flops 207622144 | bytes 9122607 | solution.py:94
  142.6 0.6 dynamic_slice.28
  144.6 4.1 %conditional.3 = ((f32[1,2,512]{2,1,0:T(2,128)S(1)}, f32[1,2,512]{2,1,0:T(2,128)S(1)}, f32[1,2,512,128]{3,2,1,0:T(8,128)S(1)})) conditional(s32[]{:T(128)} %convert_element_type.83, (f32[1,2,512]{2,1,0:T(2,128)S(1)}, f32[1,2,512]{2,1,0:T(2,128)S(1)}, f32[1,2,512,128]{3,2,1,0:T(8,128)S(1)}) %tuple.49, (s32[]{:T(128)}, s32[]{:T(128)}, ...), branch_computations={%region_2.2_spmd, %region_3.5_spmd} | conditional | flops 207622144 | bytes 9120300 | solution.py:92
  144.6 0.2 broadcast_compare_fusion
  144.8 0.9 constant_dynamic-slice_fusion
  145.7 0.6 fusion.2
  146.4 1.7 fusion.7
  148.1 0.5 fusion.6
  148.7 0.6 dynamic_slice.28
  150.7 0.6 dynamic_slice.28
  152.6 0.6 dynamic_slice.28
  154.6 0.6 dynamic_slice.28
  156.6 0.6 dynamic_slice.28
  158.5 0.6 dynamic_slice.28
  160.5 0.6 dynamic_slice.28
  162.5 0.6 dynamic_slice.28
  164.4 0.6 dynamic_slice.28
  166.4 0.6 dynamic_slice.28
  168.4 0.6 dynamic_slice.28
  170.3 0.6 dynamic_slice.28
  172.3 0.6 dynamic_slice.28
  174.3 0.6 dynamic_slice.28
  176.3 0.6 dynamic_slice.28
  178.2 0.2 broadcast_divide_fusion
  178.4 0.1 multiply_reduce_fusion
  178.6 2.4 reduce_sum.65
  181.0 0.7 copy.70
  181.7 65.2 %all-to-all-start.2 = ((bf16[16,2,24,128]{3,2,1,0:T(8,128)(2,1)}), bf16[16,2,24,128]{3,2,1,0:T(8,128)(2,1)S(1)}, u32[]{:S(2)}, u32[]{:S(2)}) async-start(bf16[16,2,24,128]{3,2,1,0:T(8,128)(2,1)} %copy.70), calls=%async_computation.2 | async-start | bytes 393216 | tf_op jit(solution)/shard_map/all_to_all | solution.py:155
  246.9 0.8 fusion.101
  247.7 6.5 %all-to-all-done.2 = bf16[16,2,24,128]{3,2,1,0:T(8,128)(2,1)S(1)} async-done(((bf16[16,2,24,128]{3,2,1,0:T(8,128)(2,1)}), bf16[16,2,24,128]{3,2,1,0:T(8,128)(2,1)S(1)}, u32[]{:S(2)}, u32[]{:S(2)}) %all-to-all-start.2) | async-done | bytes 196640 | tf_op jit(solution)/shard_map/all_to_all | solution.py:155
  254.2 1.3 gather_fusion.1
  255.5 1.1 fusion.98
  (66 shorter events, 0.4 us)
Async XLA Ops:
  7.2 75.1 %copy-start = (bf16[2,256,2048]{2,1,0:T(8,128)(2,1)S(1)}, bf16[2,256,2048]{2,1,0:T(8,128)(2,1)}, u32[]{:S(2)}) copy-start(bf16[2,256,2048]{2,1,0:T(8,128)(2,1)} %param.27) | copy-start | bytes 6291460
  7.2 23.8 %copy-start.4 = (bf16[512,1,128]{2,0,1:T(8,128)(2,1)S(1)}, bf16[512,1,128]{2,0,1:T(8,128)(2,1)}, u32[]{:S(2)}) copy-start(bf16[512,1,128]{2,0,1:T(8,128)(2,1)} %param.17) | copy-start | bytes 393220
  7.2 23.8 %copy-start.3 = (bf16[512,1,128]{2,0,1:T(8,128)(2,1)S(1)}, bf16[512,1,128]{2,0,1:T(8,128)(2,1)}, u32[]{:S(2)}) copy-start(bf16[512,1,128]{2,0,1:T(8,128)(2,1)} %param.18) | copy-start | bytes 393220
  7.2 69.3 %all-gather.5.cloned.1.call-start = ((), (), s32[]{:S(2)}) async-start(), calls=%async_computation.4 | async-start | bytes 3342336 | tf_op jit(solution)/shard_map/all_gather | solution.py:148
  8.2 68.3 %copy-start.5 = (f32[2048]{0:T(1024)S(1)}, f32[2048]{0:T(1024)}, u32[]{:S(2)}) copy-start(f32[2048]{0:T(1024)} %param.24) | copy-start | bytes 24580
  31.0 103.1 %all-gather.3.cloned.1.call-start = ((), (), s32[]{:S(2)}) async-start(), calls=%async_computation.3 | async-start | bytes 4456448 | tf_op jit(solution)/shard_map/all_gather | solution.py:22
  76.5 4.7 %copy-start.8 = (bf16[2,2048,256]{2,1,0:T(8,128)(2,1)S(1)}, bf16[2,2048,256]{2,1,0:T(8,128)(2,1)}, u32[]{:S(2)}) copy-start(bf16[2,2048,256]{2,1,0:T(8,128)(2,1)} %param.25) | copy-start | bytes 6291460
  79.5 1.7 copy-start.1
  93.1 5.3 %copy-start.6 = (f32[256,2]{0,1:T(2,128)S(1)}, f32[256,2]{0,1:T(2,128)}, u32[]{:S(2)}) copy-start(f32[256,2]{0,1:T(2,128)} %param.23) | copy-start | bytes 6148
  93.1 6.1 %copy-start.2 = (bf16[512,1,128]{2,0,1:T(8,128)(2,1)S(1)}, bf16[512,1,128]{2,0,1:T(8,128)(2,1)}, u32[]{:S(2)}) copy-start(bf16[512,1,128]{2,0,1:T(8,128)(2,1)} %param.16) | copy-start | bytes 393220
  93.1 85.5 %all-to-all-start.1 = ((bf16[16,16,2,24,128]{4,3,1,2,0:T(8,128)(2,1)}), bf16[16,16,2,24,128]{4,3,1,2,0:T(8,128)(2,1)}, u32[]{:S(2)}, u32[]{:S(2)}) async-start(bf16[16,16,2,24,128]{4,3,1,2,0:T(8,128)(2,1)} %bitcast.149), calls=%async_computation.1 | async-start | bytes 6291456 | tf_op jit(solution)/shard_map/all_to_all | solution.py:32
  178.6 68.3 %copy-start.7 = (f32[128]{0:T(128)S(1)}, f32[128]{0:T(128)}, u32[]{:S(2)}) copy-start(f32[128]{0:T(128)} %param.20) | copy-start | bytes 1540
  181.7 72.5 %all-to-all-start.2 = ((bf16[16,2,24,128]{3,2,1,0:T(8,128)(2,1)}), bf16[16,2,24,128]{3,2,1,0:T(8,128)(2,1)S(1)}, u32[]{:S(2)}, u32[]{:S(2)}) async-start(bf16[16,2,24,128]{3,2,1,0:T(8,128)(2,1)} %copy.70), calls=%async_computation.2 | async-start | bytes 393216 | tf_op jit(solution)/shard_map/all_to_all | solution.py:155
Sparse Core Ops, SparseCore 0:
  31.1 45.3 all-gather.4
  78.9 55.0 all-gather.2
where the time goes:
time: 265 us; the launch traced here: 263 us
  waiting for transfers between devices  85.2 us (32%)
  starting transfers between devices  70.6 us (27%)
  local copies, waits for them, and re-layouts  34.8 us (13%)
  loops' own time  21.6 us (8%)
  between operations  15 us (6%)
  blocking collectives  14.7 us (6%)
  other arithmetic  11.9 us (4%)
  matrix products  9.7 us (4%)
    all_to_all x1, starting transfers between devices, route_layer(): lax.all_to_all(summed, 'ep', split_axis=0, concat_axis=0, tiled=True)  65.2 us
    all_gather x1, waiting for transfers between devices, route_layer(): lax.all_gather(arrived, 'tp', axis=3, tiled=True).astype(jnp.float32)  44.7 us
    all_gather x1, waiting for transfers between devices, side_by_side(): lax.all_gather(both, axis, axis=dim, tiled=True)  34 us
    another operation x1, loops' own time, attend(): lax.scan(key_step, initial, (key_blocks, value_blocks, lax.iota(jnp.int32...  21.4 us
    all_to_all x1, blocking collectives, route_layer(): lax.all_to_all(outgoing, 'ep', split_axis=0, concat_axis=0, tiled=True)  14.7 us
    dynamic_slice x17, local copies, waits for them, and re-layouts, attend(): lax.scan(key_step, initial, (key_blocks, value_blocks, lax.iota(jnp.int32...  10.8 us
    unnamed x22, local copies, waits for them, and re-layouts  6.83 us
    all_to_all x1, waiting for transfers between devices, route_layer(): lax.all_to_all(summed, 'ep', split_axis=0, concat_axis=0, tiled=True)  6.49 us
  transfers between devices with their start and end apart: 4, of which 3 were waited for; matrix products, arithmetic and copies ran while one was open for 15% of the time, Pallas kernels for 0%

commit v1 on v0

v1 whole, which is shorter than its diff:
```python
import functools
import math

import jax
import jax.numpy as jnp
from jax import lax
from jax.experimental import pallas as pl
from jax.experimental.pallas import tpu as pltpu
from jax.sharding import PartitionSpec as P

MESH = pl.DeviceIdType.MESH
NEG_FILL = -1e30
SUB_EPS = 1e-05
NORM_EPS = 1e-06
CLAMP_LIMIT = 7.0
GLU_ALPHA = 1.702
OUT_SCALE = 0.8
AG_CUTS = 4
F32 = jnp.float32
BF16 = jnp.bfloat16


def nt_dot(a, b):
    return lax.dot_general(a, b, (((1,), (1,)), ((), ())), preferred_element_type=F32)


def tn_dot(a, b):
    return lax.dot_general(a, b, (((0,), (0,)), ((), ())), preferred_element_type=F32)


def nn_dot(a, b):
    return jnp.dot(a, b, preferred_element_type=F32)


def kernel(
    cfg,
    q_ref,
    k_ref,
    v_ref,
    mix_ref,
    sub_gain_ref,
    tokens_ref,
    routes_ref,
    pick_weight_ref,
    gain_ref,
    gate_hbm,
    up_hbm,
    down_hbm,
    attn_ref,
    moe_ref,
    qz,
    kbuf,
    vbuf,
    acc,
    row_max,
    picks,
    outgoing,
    gathered,
    gate_w,
    up_w,
    down_w,
    pre,
    squares,
    hidden,
    ybuf,
    prec,
    rsend,
    rrecv,
    back_send,
    back,
    w_sem,
    k_send,
    k_recv,
    v_send,
    v_recv,
    d_send,
    d_recv,
    g_send,
    g_recv,
    p_send,
    p_recv,
    y_send,
    y_recv,
    r_send,
    r_recv,
    b_send,
    b_recv,
):
    n_ep, n_tp, cap, rows = cfg["n_ep"], cfg["n_tp"], cfg["cap"], cfg["rows"]
    n_z = n_tp // 2
    block = 2 * cap
    slots = n_ep * block
    half = slots // 2
    sources_half = n_ep // 2
    per_expert = half // 2
    ep = lax.axis_index("ep")
    tp = lax.axis_index("tp")
    z, c = lax.div(tp, 2), lax.rem(tp, 2)
    partner = tp + 1 - 2 * c

    def ring(at, shift):
        return lax.rem(at + shift + 2 * n_z, n_z)

    def remote(src, dst, send_sem, recv_sem, to_ep, to_tp):
        return pltpu.make_async_remote_copy(
            src_ref=src,
            dst_ref=dst,
            send_sem=send_sem,
            recv_sem=recv_sem,
            device_id=(to_ep, to_tp),
            device_id_type=MESH,
        )

    barrier = pltpu.get_barrier_semaphore()
    for off in range(1, n_ep):
        pl.semaphore_signal(
            barrier, inc=1, device_id=(lax.rem(ep + off, n_ep), tp), device_id_type=MESH
        )
    for to in (2 * ring(z, 1) + c, 2 * ring(z, -1) + c, partner):
        pl.semaphore_signal(barrier, inc=1, device_id=(ep, to), device_id_type=MESH)

    weight_copies = [
        pltpu.make_async_copy(gate_hbm, gate_w, w_sem.at[0]),
        pltpu.make_async_copy(up_hbm, up_w, w_sem.at[1]),
        pltpu.make_async_copy(down_hbm, down_w, w_sem.at[2]),
    ]
    for copy in weight_copies:
        copy.start()

    pairs = 2 * rows
    experts = 2 * n_ep
    routes = routes_ref[...]
    member = (
        lax.broadcasted_iota(jnp.int32, (experts, pairs), 0)
        == jnp.broadcast_to(routes, (experts, pairs))
    ).astype(F32)

    def order(dim):
        at = lax.broadcasted_iota(jnp.int32, (pairs, pairs), dim)
        return jnp.where(at < rows, 2 * at, 2 * (at - rows) + 1)

    earlier = (order(0) < order(1)).astype(F32).astype(BF16)
    rank = nn_dot(member.astype(BF16), earlier)
    first_slot = lax.broadcasted_iota(jnp.int32, (experts, pairs), 0).astype(F32) * float(cap)
    target = jnp.sum(member * (rank + first_slot), axis=0, keepdims=True)
    slot_at = lax.broadcasted_iota(jnp.int32, (slots, rows), 0).astype(F32)
    pick_0 = (slot_at == jnp.broadcast_to(target[:, :rows], (slots, rows))).astype(F32)
    pick_1 = (slot_at == jnp.broadcast_to(target[:, rows:], (slots, rows))).astype(F32)
    picks[0] = pick_0.astype(BF16)
    picks[1] = pick_1.astype(BF16)
    out_rows = nn_dot((pick_0 + pick_1).astype(BF16), tokens_ref[...]).astype(BF16)
    outgoing[...] = out_rows
    mine = pl.ds(pl.multiple_of(ep * block, block), block)
    gathered[tp, mine, :] = outgoing[mine, :]

    q_all = q_ref[...]
    q_rows = q_all.shape[0]
    lane = lax.broadcasted_iota(jnp.int32, q_all.shape, 1)
    zero = jnp.zeros_like(q_all)
    qz[:q_rows] = jnp.where(lane < q_all.shape[1] // 2, q_all, zero)
    qz[q_rows:] = jnp.where(lane >= q_all.shape[1] // 2, q_all, zero)

    pl.semaphore_wait(barrier, n_ep - 1 + 3)

    def dispatch_copy(off):
        to = lax.rem(ep + off, n_ep)
        return remote(
            outgoing.at[pl.ds(pl.multiple_of(to * block, block), block)],
            gathered.at[tp, mine],
            d_send.at[off],
            d_recv.at[off],
            to,
            tp,
        )

    for off in range(1, n_ep):
        dispatch_copy(off).start()

    def key_copy(off):
        return remote(k_ref, kbuf.at[off], k_send.at[off], k_recv.at[off], ep + off, tp)

    def value_copy(off):
        return remote(v_ref, vbuf.at[off], v_send.at[off], v_recv.at[off], ep + off, tp)

    @pl.loop(1, n_ep)
    def _(off):
        @pl.when(ep + off < n_ep)
        def _():
            key_copy(off).start()
            value_copy(off).start()

    exponent = (q_ref.shape[1] // 2) ** (-0.5) * math.log2(math.e)
    width = v_ref.shape[1]
    tile = min(256, q_rows)

    def attend(keys, values, first):
        both = jnp.concatenate([values, jnp.ones_like(values)], axis=1)
        for r in range(0, 2 * q_rows, tile):
            at = pl.ds(r, tile)
            scores = nt_dot(qz[at, :], keys)
            if first:
                seen = lax.broadcasted_iota(jnp.int32, scores.shape, 1) <= (
                    lax.broadcasted_iota(jnp.int32, scores.shape, 0) + r % q_rows
                )
                scores = jnp.where(seen, scores, NEG_FILL)
                top = jnp.broadcast_to(jnp.max(scores, axis=1, keepdims=True), (tile, 128))
            else:
                old = row_max[at, :]
                top = jnp.maximum(old, jnp.max(scores, axis=1, keepdims=True))
            weights = jnp.exp2((scores - top[:, :1]) * exponent).astype(BF16)
            part = nn_dot(weights, both)
            if first:
                acc[at, :] = part
            else:
                shrink = jnp.exp2((old - top) * exponent)
                acc[at, :] = acc[at, :] * jnp.concatenate([shrink, shrink], axis=1) + part
            row_max[at, :] = top

    def attend_step(off):
        @pl.when(ep >= off)
        def _():
            remote(k_ref, kbuf.at[off], k_send.at[off], k_recv.at[off], ep, partner).wait_recv()
            remote(v_ref, vbuf.at[off], v_send.at[off], v_recv.at[off], ep, partner).wait_recv()
            attend(kbuf[off], vbuf[off], False)

    attend(k_ref[...], v_ref[...], True)

    cut = half // AG_CUTS

    def gather_copy(h, hop, sub):
        source = ring(z, -hop) if h == 0 else ring(z, hop)
        to = ring(z, 1) if h == 0 else ring(z, -1)
        piece = gathered.at[2 * source + c, pl.ds(h * half + sub * cut, cut)]
        at = (h * n_z + hop) * AG_CUTS + sub
        return remote(piece, piece, g_send.at[at], g_recv.at[at], ep, 2 * to + c)

    def gather_wait(h, hop, sub):
        source = ring(z, -hop) if h == 0 else ring(z, hop)
        piece = gathered.at[2 * source + c, pl.ds(h * half + sub * cut, cut)]
        at = (h * n_z + hop - 1) * AG_CUTS + sub
        remote(piece, piece, g_send.at[at], g_recv.at[at], ep, partner).wait_recv()

    def partner_copy(h, hop, mine_or_theirs):
        source = ring(z, -hop) if h == 0 else ring(z, hop)
        piece = gathered.at[2 * source + mine_or_theirs, pl.ds(h * half, half)]
        at = h * n_z + hop
        return remote(piece, piece, p_send.at[at], p_recv.at[at], ep, partner)

    for h in range(2):
        for s in range(h * sources_half, (h + 1) * sources_half):

            @pl.when(ep != s)
            def _(s=s):
                off = lax.rem(ep - s + n_ep, n_ep)
                piece = gathered.at[tp, pl.ds(s * block, block)]
                remote(piece, piece, d_send.at[off], d_recv.at[off], s, tp).wait_recv()

        for sub in range(AG_CUTS):
            gather_copy(h, 0, sub).start()
        partner_copy(h, 0, c).start()

    for copy in weight_copies:
        copy.wait()

    def by_expert(value):
        w = value.shape[1]
        cut_up = value.reshape(sources_half, 2, cap, w)
        return [cut_up[:, e].reshape(per_expert, w) for e in range(2)]

    def expert_in(hop, first):
        for h in range(2):
            source = ring(z, -hop) if h == 0 else ring(z, hop)
            partner_copy(h, hop, 1 - c).wait_recv()
            at = pl.ds(h * half, half)
            x = jnp.concatenate(
                [gathered[2 * source, at, :], gathered[2 * source + 1, at, :]], axis=1
            ).astype(F32)
            square = jnp.broadcast_to(jnp.sum(x * x, axis=1, keepdims=True), (half, 128))
            squares[h] = square if first else squares[h] + square
            depth = x.shape[1]
            deep = pl.ds(pl.multiple_of(source * depth, depth), depth)
            for e, rows_e in enumerate(by_expert(x * gain_ref[source])):
                rows_e = rows_e.astype(BF16)
                for n, w in enumerate((gate_w, up_w)):
                    product = nn_dot(rows_e, w[e, deep, :])
                    pre[h, e, n] = product if first else pre[h, e, n] + product

    for hop in range(1, n_z):
        for sub in range(AG_CUTS):
            for h in range(2):
                gather_wait(h, hop, sub)
                if hop < n_z - 1:
                    gather_copy(h, hop, sub).start()
        for h in range(2):
            partner_copy(h, hop, c).start()
        expert_in(hop - 1, hop == 1)
    expert_in(n_z - 1, False)

    for h in range(2):
        factor = lax.rsqrt(squares[h] / float(cfg["width"]) + NORM_EPS)
        for e, f in enumerate(by_expert(factor)):
            f = jnp.concatenate([f, f], axis=1)
            gate = jnp.minimum(pre[h, e, 0] * f, CLAMP_LIMIT)
            up = jnp.clip(pre[h, e, 1] * f, -CLAMP_LIMIT, CLAMP_LIMIT)
            hidden[h, e] = ((up + 1.0) * gate * jax.nn.sigmoid(GLU_ALPHA * gate)).astype(BF16)

    def down(hop):
        for h in range(2):
            goal = ring(z, -1 - hop) if h == 0 else ring(z, 1 + hop)
            wide = pl.ds(pl.multiple_of(goal * 256, 256), 256)
            for e in range(2):
                y = nn_dot(hidden[h, e], down_w[e, :, wide]).astype(BF16)
                ybuf[0, h, hop, e] = y[:, :128]
                ybuf[1, h, hop, e] = y[:, 128:]

    def y_copy(h, hop):
        at = h * n_z + hop
        return remote(
            ybuf.at[1 - c, h, hop], prec.at[h, hop], y_send.at[at], y_recv.at[at], ep, partner
        )

    def sum_copy(h, hop, e):
        to = ring(z, 1) if h == 0 else ring(z, -1)
        at = (h * n_z + hop) * 2 + e
        return remote(
            rsend.at[h, hop, e], rrecv.at[h, hop, e], r_send.at[at], r_recv.at[at], ep, 2 * to + c
        )

    def own_sum(h, hop, e):
        return ybuf[c, h, hop, e].astype(F32) + prec[h, hop, e].astype(F32)

    for hop in range(n_z):
        down(hop)
        for h in range(2):
            y_copy(h, hop).start()
    for h in range(2):
        y_copy(h, 0).wait_recv()
        for e in range(2):
            rsend[h, 0, e] = own_sum(h, 0, e).astype(BF16)
            sum_copy(h, 0, e).start()

    @pl.loop(1, n_ep)
    def _(off):
        attend_step(off)

    for hop in range(1, n_z - 1):
        for h in range(2):
            y_copy(h, hop).wait_recv()
        for e in range(2):
            for h in range(2):
                sum_copy(h, hop - 1, e).wait_recv()
                total = own_sum(h, hop, e) + rrecv[h, hop - 1, e].astype(F32)
                rsend[h, hop, e] = total.astype(BF16)
                sum_copy(h, hop, e).start()

    def back_copy(s):
        off = lax.rem(s - ep + n_ep, n_ep)
        return remote(
            back_send.at[pl.ds(s * block, block)],
            back.at[mine],
            b_send.at[off],
            b_recv.at[off],
            s,
            tp,
        )

    last = n_z - 1
    for h in range(2):
        y_copy(h, last).wait_recv()
        totals = []
        for e in range(2):
            sum_copy(h, last - 1, e).wait_recv()
            total = own_sum(h, last, e) + rrecv[h, last - 1, e].astype(F32)
            totals.append(total.reshape(sources_half, 1, cap, 128))
        back_send[h * half : (h + 1) * half] = (
            jnp.concatenate(totals, axis=1).reshape(half, 128).astype(BF16)
        )
        for s in range(h * sources_half, (h + 1) * sources_half):

            @pl.when(ep != s)
            def _(s=s):
                back_copy(s).start()

    back[mine, :] = back_send[mine, :]

    mix = mix_ref[0, 0]
    for r in range(0, q_rows, tile):
        one, two = pl.ds(r, tile), pl.ds(q_rows + r, tile)
        blend = acc[one, :width] / acc[one, width:] - mix * (acc[two, :width] / acc[two, width:])
        mean = jnp.mean(blend * blend, axis=1, keepdims=True)
        scaled = blend * lax.rsqrt(mean + SUB_EPS)
        attn_ref[one, :] = (scaled * sub_gain_ref[...] * OUT_SCALE).astype(BF16)

    for off in range(1, n_ep):
        piece = back.at[mine]
        remote(piece, piece, b_send.at[off], b_recv.at[off], ep, partner).wait_recv()
    result = back[...]
    weight = pick_weight_ref[...]
    moe_ref[...] = (
        tn_dot(picks[0], result) * weight[:, :1] + tn_dot(picks[1], result) * weight[:, 1:]
    ).astype(BF16)

    for off in range(1, n_ep):
        dispatch_copy(off).wait_send()
        back_copy(lax.rem(ep + off, n_ep)).wait_send()

    @pl.loop(1, n_ep)
    def _(off):
        @pl.when(ep + off < n_ep)
        def _():
            key_copy(off).wait_send()
            value_copy(off).wait_send()

    for h in range(2):
        for hop in range(n_z):
            partner_copy(h, hop, c).wait_send()
            y_copy(h, hop).wait_send()
            if hop < n_z - 1:
                for sub in range(AG_CUTS):
                    gather_copy(h, hop, sub).wait_send()
                for e in range(2):
                    sum_copy(h, hop, e).wait_send()


def shards(
    queries,
    keys,
    values,
    mix_weight,
    sub_gain,
    tokens,
    routes,
    route_weights,
    expert_gain,
    gate_weight,
    up_weight,
    down_weight,
):
    n_ep, n_tp = lax.axis_size("ep"), lax.axis_size("tp")
    n_z = n_tp // 2
    rows, pick_count = routes.shape
    experts = n_ep * gate_weight.shape[0]
    cap = 3 * rows * pick_count // (2 * experts)
    slots = experts * cap
    half = slots // 2
    q_rows, _, qk_width = queries.shape
    v_width = values.shape[2]
    width = expert_gain.shape[0]
    ff = gate_weight.shape[2]
    cfg = dict(n_ep=n_ep, n_tp=n_tp, cap=cap, rows=rows, width=width)
    dma = pltpu.SemaphoreType.DMA
    vmem = pl.BlockSpec(memory_space=pltpu.VMEM)
    anywhere = pl.BlockSpec(memory_space=pl.ANY)
    attn_out, moe_out = pl.pallas_call(
        functools.partial(kernel, cfg),
        name="layer",
        out_shape=(
            jax.ShapeDtypeStruct((q_rows, v_width), BF16),
            jax.ShapeDtypeStruct((rows, tokens.shape[1]), BF16),
        ),
        in_specs=[vmem] * 3
        + [pl.BlockSpec(memory_space=pltpu.SMEM)]
        + [vmem] * 5
        + [anywhere] * 3,
        out_specs=(vmem, vmem),
        scratch_shapes=[
            pltpu.VMEM((2 * q_rows, qk_width), BF16),
            pltpu.VMEM((n_ep, q_rows, qk_width), BF16),
            pltpu.VMEM((n_ep, q_rows, v_width), BF16),
            pltpu.VMEM((2 * q_rows, 2 * v_width), F32),
            pltpu.VMEM((2 * q_rows, 128), F32),
            pltpu.VMEM((2, slots, rows), BF16),
            pltpu.VMEM((slots, tokens.shape[1]), BF16),
            pltpu.VMEM((n_tp, slots, tokens.shape[1]), BF16),
            pltpu.VMEM(gate_weight.shape, BF16),
            pltpu.VMEM(up_weight.shape, BF16),
            pltpu.VMEM(down_weight.shape, BF16),
            pltpu.VMEM((2, 2, 2, half // 2, ff), F32),
            pltpu.VMEM((2, half, 128), F32),
            pltpu.VMEM((2, 2, half // 2, ff), BF16),
            pltpu.VMEM((2, 2, n_z, 2, half // 2, 128), BF16),
            pltpu.VMEM((2, n_z, 2, half // 2, 128), BF16),
            pltpu.VMEM((2, n_z - 1, 2, half // 2, 128), BF16),
            pltpu.VMEM((2, n_z - 1, 2, half // 2, 128), BF16),
            pltpu.VMEM((slots, 128), BF16),
            pltpu.VMEM((slots, 128), BF16),
            dma((3,)),
            dma((n_ep,)),
            dma((n_ep,)),
            dma((n_ep,)),
            dma((n_ep,)),
            dma((n_ep,)),
            dma((n_ep,)),
            dma((2 * n_z * AG_CUTS,)),
            dma((2 * n_z * AG_CUTS,)),
            dma((2 * n_z,)),
            dma((2 * n_z,)),
            dma((2 * n_z,)),
            dma((2 * n_z,)),
            dma((2 * n_z * 2,)),
            dma((2 * n_z * 2,)),
            dma((n_ep,)),
            dma((n_ep,)),
        ],
        compiler_params=pltpu.CompilerParams(
            collective_id=0, has_side_effects=True, vmem_limit_bytes=60 * 1024 * 1024
        ),
    )(
        queries.reshape(q_rows, qk_width),
        keys.reshape(q_rows, qk_width),
        values.reshape(q_rows, v_width),
        mix_weight.reshape(1, 1),
        sub_gain.reshape(1, v_width),
        tokens,
        routes.T.reshape(1, 2 * rows),
        route_weights,
        expert_gain.reshape(n_z, 1, width // n_z),
        gate_weight,
        up_weight,
        down_weight,
    )
    return attn_out.reshape(q_rows, 1, v_width), moe_out


def solution(mesh):
    return jax.shard_map(
        shards,
        mesh=mesh,
        in_specs=(
            P("ep", "tp", None),
            P("ep", "tp", None),
            P("ep", "tp", None),
            P("tp"),
            P(),
            P("ep", "tp"),
            P("ep", None),
            P("ep", None),
            P(),
            P("ep", None, "tp"),
            P("ep", None, "tp"),
            P("ep", "tp", None),
        ),
        out_specs=(P("ep", "tp", None), P("ep", "tp")),
        check_vma=False,
    )
```

time: 265 us -> 121 us (0.46)
  Pallas kernels: 0 us -> 112 us
  waiting for transfers between devices: 85.2 us -> 0 us
  starting transfers between devices: 70.6 us -> 0 us
  local copies, waits for them, and re-layouts: 34.8 us -> 5.78 us
  loops' own time: 21.6 us -> 0 us
  blocking collectives: 14.7 us -> 0 us
  between operations: 15 us -> 1.29 us
  other arithmetic: 11.9 us -> 0 us
  matrix products: 9.7 us -> 0 us
    pallas_call x0 -> x1, Pallas kernels: none -> 112 us  [shards(): pl.pallas_call(functools.partial(kernel, cfg), name='layer', out_shape=(j...]
    all_gather x2 -> x0, waiting for transfers between devices: 78.7 us -> none  [the longest x1 44.7 us: route_layer(): lax.all_gather(arrived, 'tp', axis=3, tiled=True).astype(jnp.float32)]
    all_to_all x2 -> x0, starting transfers between devices: 70.5 us -> none  [the longest x1 65.2 us: route_layer(): lax.all_to_all(summed, 'ep', split_axis=0, concat_axis=0, tiled=True)]
    another operation x17 -> x0, loops' own time: 21.6 us -> none  [the longest x1 21.4 us: attend(): lax.scan(key_step, initial, (key_blocks, value_blocks, lax.iota(jnp.int32...]
    all_to_all x1 -> x0, blocking collectives: 14.7 us -> none  [route_layer(): lax.all_to_all(outgoing, 'ep', split_axis=0, concat_axis=0, tiled=True)]
    dynamic_slice x17 -> x0, local copies, waits for them, and re-layouts: 10.8 us -> none  [attend(): lax.scan(key_step, initial, (key_blocks, value_blocks, lax.iota(jnp.int32...]
    dot_general x4 -> x0, matrix products: 9.7 us -> none  [the longest x1 6.28 us: expert_finish(): jnp.einsum('secf,efd->secd', hidden, down_weight, preferred_element_type=...]
    reduce_sum x6 -> x0, other arithmetic: 7.23 us -> none  [the longest x1 3.05 us: route_layer(): squares = jnp.sum(floats * floats, axis=-1)]
  transfers between devices with their start and end apart: 4 -> 0, of which waited for: 3 -> 0; matrix products, arithmetic and copies ran while one was open for 15% -> 0% of each run, Pallas kernels for 0% -> 0%
where the time goes in v1:
time: 121 us; the launch traced here: 119 us
  Pallas kernels  112 us (93%)
  local copies, waits for them, and re-layouts  5.78 us (5%)
  between operations  1.29 us (1%)
    pallas_call x1, Pallas kernels, shards(): pl.pallas_call(functools.partial(kernel, cfg), name='layer', out_shape=(j...  112 us
    unnamed x4, local copies, waits for them, and re-layouts  5.78 us

profile of v1, /device:TPU:1, one launch (start us, length us, event | category | flops | bytes accessed | tf_op | source)
XLA Modules:
  0.0 119.0 jit_solution(4585202574244780947)
XLA Ops:
  1.3 1.3 %copy.15 = s32[1,1,2,256]{3,1,2,0:T(1,128)} copy(s32[1,1,2,256]{3,2,1,0:T(2,128)} %bitcast.18) | data formatting | bytes 4096
  2.5 1.5 %copy.14.pick_weight_ref = f32[256,2]{1,0:T(8,128)} copy(f32[256,2]{0,1:T(2,128)} %param.19) | data formatting | bytes 4096 | tf_op args[7]
  4.0 112.0 %layer.1 = (bf16[512,128]{1,0:T(8,128)(2,1)}, bf16[256,128]{1,0:T(8,128)(2,1)}) custom-call(bf16[512,128]{1,0:T(8,128)(2,1)} %bitcast.12, bf16[512,128]{1,0:T(8,128)(2,1)} %bitcast.13, bf16[512,128]{1,0:T(8,128)(2,1)} %bitcast.14, f32[1,1]{1,0:T(1,128)} %bitcast.11.mix_ref, f32[1,128]{1,0:T(1,128)} %bitcast.19, bf16[256,128]{1,0:T(8,128)(2,1)} %tokens_ref.1, ...), custom_call_target="tpu_custom_call" | custom-call | tf_op jit(solution)/shard_map/layer/pallas_call | solution.py:454
  116.0 1.6 %copy.19 = bf16[512,1,128]{2,0,1:T(8,128)(2,1)} copy(bf16[512,1,128]{2,0,1:T(8,128)(2,1)} %bitcast.15) | data formatting | bytes 262144
  117.5 1.5 %copy.20 = bf16[256,128]{1,0:T(8,128)(2,1)} copy(bf16[256,128]{1,0:T(8,128)(2,1)} %get-tuple-element.9) | data formatting | bytes 131072

commit v2 on v1

v2 whole, which is shorter than its diff:
```python
import functools
import math

import jax
import jax.numpy as jnp
from jax import lax
from jax.experimental import pallas as pl
from jax.experimental.pallas import tpu as pltpu
from jax.sharding import PartitionSpec as P

MESH = pl.DeviceIdType.MESH
NEG_FILL = -1e30
SUB_EPS = 1e-05
NORM_EPS = 1e-06
CLAMP_LIMIT = 7.0
GLU_ALPHA = 1.702
OUT_SCALE = 0.8
F32 = jnp.float32
BF16 = jnp.bfloat16


def nt_dot(a, b):
    return lax.dot_general(a, b, (((1,), (1,)), ((), ())), preferred_element_type=F32)


def tn_dot(a, b):
    return lax.dot_general(a, b, (((0,), (0,)), ((), ())), preferred_element_type=F32)


def nn_dot(a, b):
    return jnp.dot(a, b, preferred_element_type=F32)


STAGES = (
    ((), (((0, 0), "x+"), ((0, 0), "x-"), ((0, 0), "y+"), ((0, 0), "y-"))),
    (
        ((0, -1), (0, 1), (-1, 0), (1, 0)),
        (
            ((0, -1), "x+"),
            ((0, -1), "y+"),
            ((0, -1), "y-"),
            ((0, 1), "y+"),
            ((0, 1), "y-"),
            ((-1, 0), "y+"),
        ),
    ),
    (
        ((0, 2), (-1, -1), (1, -1), (-1, 1), (1, 1), (2, 0)),
        (((0, 2), "y+"), ((0, 2), "y-"), ((-1, -1), "y+"), ((1, 1), "y-")),
    ),
    (((-1, 2), (1, 2), (2, -1), (2, 1)), (((1, 2), "y-"),)),
    (((2, 2),), ()),
)
STEP = {"x+": (0, 1), "x-": (0, -1), "y+": (1, 0), "y-": (-1, 0)}
MIRROR = {"x+": "y-", "x-": "y+", "y+": "x-", "y-": "x+"}
SIDE = 4


def kernel(
    cfg,
    q_hbm,
    k_hbm,
    v_hbm,
    mix_hbm,
    sub_gain_hbm,
    tokens_hbm,
    routes_hbm,
    pick_weight_hbm,
    gain_hbm,
    gate_hbm,
    up_hbm,
    down_hbm,
    attn_hbm,
    moe_hbm,
    q_ref,
    mix_ref,
    sub_gain_ref,
    tokens_ref,
    routes_ref,
    pick_weight_ref,
    gain_ref,
    gate_w,
    up_w,
    down_w,
    attn_ref,
    moe_ref,
    qz,
    kbuf,
    vbuf,
    acc,
    row_max,
    picks,
    outgoing,
    gathered,
    pre,
    squares,
    hidden,
    ybuf,
    prec,
    rsend,
    rrecv,
    back_send,
    back,
    in_sem,
    out_sem,
    kv_send,
    kv_recv,
    d_sem,
    g_send,
    g_recv,
    p_send,
    p_recv,
    y_send,
    y_recv,
    r_send,
    r_recv,
    b_sem,
):
    n_ep, n_tp, cap, rows = cfg["n_ep"], cfg["n_tp"], cfg["cap"], cfg["rows"]
    n_z = n_tp // 2
    far = n_z // 2
    block = 2 * cap
    slots = n_ep * block
    half = slots // 2
    sources_half = n_ep // 2
    part = half // 2
    ep = lax.axis_index("ep")
    tp = lax.axis_index("tp")
    z, c = lax.div(tp, 2), lax.rem(tp, 2)
    py, px = lax.div(ep, SIDE), lax.rem(ep, SIDE)
    partner = tp + 1 - 2 * c

    def ring(at, shift):
        return lax.rem(at + shift + 2 * n_z, n_z)

    def remote(src, dst, send_sem, recv_sem, to_ep, to_tp):
        return pltpu.make_async_remote_copy(
            src_ref=src,
            dst_ref=dst,
            send_sem=send_sem,
            recv_sem=recv_sem,
            device_id=(to_ep, to_tp),
            device_id_type=MESH,
        )

    barrier = pltpu.get_barrier_semaphore()
    for off in range(1, n_ep):
        pl.semaphore_signal(
            barrier, inc=1, device_id=(lax.rem(ep + off, n_ep), tp), device_id_type=MESH
        )
    for to in (2 * ring(z, 1) + c, 2 * ring(z, -1) + c, partner):
        pl.semaphore_signal(barrier, inc=1, device_id=(ep, to), device_id_type=MESH)

    loads = [
        pltpu.make_async_copy(src, dst, in_sem.at[i])
        for i, (src, dst) in enumerate(
            (
                (routes_hbm, routes_ref),
                (tokens_hbm, tokens_ref),
                (q_hbm, q_ref),
                (k_hbm, kbuf.at[0]),
                (v_hbm, vbuf.at[0]),
                (gain_hbm, gain_ref),
                (gate_hbm, gate_w),
                (up_hbm, up_w),
                (down_hbm, down_w),
                (mix_hbm, mix_ref),
                (sub_gain_hbm, sub_gain_ref),
                (pick_weight_hbm, pick_weight_ref),
            )
        )
    ]
    for copy in loads:
        copy.start()

    for copy in loads[:2]:
        copy.wait()
    pairs = 2 * rows
    experts = 2 * n_ep
    routes = jnp.concatenate([routes_ref[0:1, :], routes_ref[1:2, :]], axis=1)
    member = (
        lax.broadcasted_iota(jnp.int32, (experts, pairs), 0)
        == jnp.broadcast_to(routes, (experts, pairs))
    ).astype(F32)

    def order(dim):
        at = lax.broadcasted_iota(jnp.int32, (pairs, pairs), dim)
        return jnp.where(at < rows, 2 * at, 2 * (at - rows) + 1)

    earlier = (order(0) < order(1)).astype(F32).astype(BF16)
    rank = nn_dot(member.astype(BF16), earlier)
    first_slot = lax.broadcasted_iota(jnp.int32, (experts, pairs), 0).astype(F32) * float(cap)
    target = jnp.sum(member * (rank + first_slot), axis=0, keepdims=True)
    slot_at = lax.broadcasted_iota(jnp.int32, (slots, rows), 0).astype(F32)
    pick_0 = (slot_at == jnp.broadcast_to(target[:, :rows], (slots, rows))).astype(F32)
    pick_1 = (slot_at == jnp.broadcast_to(target[:, rows:], (slots, rows))).astype(F32)
    picks[0] = pick_0.astype(BF16)
    picks[1] = pick_1.astype(BF16)
    out_rows = nn_dot((pick_0 + pick_1).astype(BF16), tokens_ref[...]).astype(BF16)
    outgoing[...] = out_rows
    mine = pl.ds(pl.multiple_of(ep * block, block), block)
    gathered[tp, mine, :] = outgoing[mine, :]

    loads[2].wait()
    q_all = q_ref[...]
    q_rows = q_all.shape[0]
    lane = lax.broadcasted_iota(jnp.int32, q_all.shape, 1)
    zero = jnp.zeros_like(q_all)
    qz[:q_rows] = jnp.where(lane < q_all.shape[1] // 2, q_all, zero)
    qz[q_rows:] = jnp.where(lane >= q_all.shape[1] // 2, q_all, zero)

    pl.semaphore_wait(barrier, n_ep - 1 + 3)

    for off in range(1, n_ep):
        to = lax.rem(ep + off, n_ep)
        remote(
            outgoing.at[pl.ds(pl.multiple_of(to * block, block), block)],
            gathered.at[tp, mine],
            d_sem.at[0],
            d_sem.at[1],
            to,
            tp,
        ).start()
    others = (n_ep - 1) * block

    exponent = (q_ref.shape[1] // 2) ** (-0.5) * math.log2(math.e)
    width = vbuf.shape[2]
    tile = min(256, q_rows)

    def scores_at(r, keys, first):
        scores = nt_dot(qz[pl.ds(r, tile), :], keys)
        if first:
            seen = lax.broadcasted_iota(jnp.int32, scores.shape, 1) <= (
                lax.broadcasted_iota(jnp.int32, scores.shape, 0) + r % q_rows
            )
            scores = jnp.where(seen, scores, NEG_FILL)
        return scores

    def attend(held, maps=(0, 1), first=False):
        keys = jnp.concatenate([kbuf[s] for s in held], axis=0)
        values = jnp.concatenate([vbuf[s] for s in held], axis=0)
        both = jnp.concatenate([values, jnp.ones_like(values)], axis=1)
        at = [m * q_rows + r for m in maps for r in range(0, q_rows, tile)]
        scores = [scores_at(r, keys, first) for r in at]
        tops = [jnp.max(s, axis=1, keepdims=True) for s in scores]
        if first:
            tops = [jnp.broadcast_to(t, (tile, 128)) for t in tops]
        else:
            olds = [row_max[pl.ds(r, tile), :] for r in at]
            tops = [jnp.maximum(o, t) for o, t in zip(olds, tops)]
        weights = [
            jnp.exp2((s - t[:, :1]) * exponent).astype(BF16) for s, t in zip(scores, tops)
        ]
        for i, r in enumerate(at):
            where = pl.ds(r, tile)
            added = nn_dot(weights[i], both)
            if first:
                acc[where, :] = added
            else:
                shrink = jnp.exp2((olds[i] - tops[i]) * exponent)
                acc[where, :] = acc[where, :] * jnp.concatenate([shrink, shrink], axis=1) + added
            row_max[where, :] = tops[i]

    def held_at(a, b):
        return (a % SIDE) * SIDE + b % SIDE

    def spread(stage):
        waits, sends = STAGES[stage]
        for n, buf in enumerate((kbuf, vbuf)):
            for a, b in waits:
                at = held_at(a, b) if n == 0 else held_at(-b, -a)
                remote(
                    buf.at[at], buf.at[at], kv_send.at[n], kv_recv.at[n, at], ep, partner
                ).wait_recv()
        for (a, b), way in sends:
            for n, buf in enumerate((kbuf, vbuf)):
                if n == 1:
                    a, b, way = -b, -a, MIRROR[way]
                dy, dx = STEP[way]
                to = lax.rem(py + dy + SIDE, SIDE) * SIDE + lax.rem(px + dx + SIDE, SIDE)
                at = held_at(a - dy, b - dx)
                remote(
                    buf.at[held_at(a, b)], buf.at[at], kv_send.at[n], kv_recv.at[n, at], to, tp
                ).start()

    for copy in loads[3:5]:
        copy.wait()
    attend((0,), first=True)
    spread(0)

    arrived = gathered.at[tp, pl.ds(0, others)]
    remote(arrived, arrived, d_sem.at[0], d_sem.at[1], ep, partner).wait_recv()

    cut = half // 2

    def source_of(way, hop):
        return ring(z, -hop) if way == 0 else ring(z, hop)

    def gather_copy(way, hop, sub):
        to = ring(z, 1) if way == 0 else ring(z, -1)
        piece = gathered.at[2 * source_of(way, hop) + c, pl.ds(sub * cut, cut)]
        at = (way * far + hop) * 4 + sub
        return remote(piece, piece, g_send.at[0], g_recv.at[at], ep, 2 * to + c)

    def gather_wait(way, hop, sub):
        piece = gathered.at[2 * source_of(way, hop) + c, pl.ds(sub * cut, cut)]
        at = (way * far + hop - 1) * 4 + sub
        remote(piece, piece, g_send.at[0], g_recv.at[at], ep, partner).wait_recv()

    def subs_of(way, hop):
        return range(4) if hop < far - 1 else range(2 * way, 2 * way + 2)

    def shard(way, hop):
        return 0 if hop == 0 else (2 * hop - 1 + way if hop < far else n_z - 1)

    def partner_copy(way, hop, h, core):
        piece = gathered.at[2 * source_of(way, hop) + core, pl.ds(h * half, half)]
        return remote(
            piece, piece, p_send.at[0], p_recv.at[shard(way, hop) * 2 + h], ep, partner
        )

    for sub in range(4):
        for way in range(2):
            if sub in subs_of(way, 0):
                gather_copy(way, 0, sub).start()
    for h in range(2):
        partner_copy(0, 0, h, c).start()

    def by_expert(value):
        w = value.shape[1]
        cut_up = value.reshape(sources_half, 2, cap, w)
        return [cut_up[:, e].reshape(part, w) for e in range(2)]

    def expert_in(way, hop, h):
        source = source_of(way, hop)
        partner_copy(way, hop, h, 1 - c).wait_recv()
        at = pl.ds(h * half, half)
        x = jnp.concatenate(
            [gathered[2 * source, at, :], gathered[2 * source + 1, at, :]], axis=1
        ).astype(F32)
        square = jnp.broadcast_to(jnp.sum(x * x, axis=1, keepdims=True), (half, 128))
        squares[h] = square if hop == 0 else squares[h] + square
        depth = x.shape[1]
        deep = pl.ds(pl.multiple_of(source * depth, depth), depth)
        for e, rows_e in enumerate(by_expert(x * gain_ref[source])):
            rows_e = rows_e.astype(BF16)
            for n, w in enumerate((gate_w, up_w)):
                product = nn_dot(rows_e, w[e, deep, :])
                pre[h, e, n] = product if hop == 0 else pre[h, e, n] + product

    for copy in loads[5:]:
        copy.wait()
    spread(1)

    for hop in range(1, far + 1):
        for step in range(4 if hop < far else 2):
            for way in range(2):
                sub = step if hop < far else 2 * way + step
                gather_wait(way, hop, sub)
                if hop < far and sub in subs_of(way, hop):
                    gather_copy(way, hop, sub).start()
            if step % 2 == 1:
                h = step // 2
                for way in range(2):
                    if hop < far:
                        partner_copy(way, hop, h, c).start()
                    else:
                        partner_copy(way, hop, way, c).start()
                for half_at in (h,) if hop < far else (0, 1):
                    expert_in(0, hop - 1, half_at)
                    if hop > 1:
                        expert_in(1, hop - 1, half_at)
    for way in range(2):
        expert_in(way, far, way)

    for h in range(2):
        factor = lax.rsqrt(squares[h] / float(cfg["width"]) + NORM_EPS)
        for e, f in enumerate(by_expert(factor)):
            f = jnp.concatenate([f, f], axis=1)
            gate = jnp.minimum(pre[h, e, 0] * f, CLAMP_LIMIT)
            up = jnp.clip(pre[h, e, 1] * f, -CLAMP_LIMIT, CLAMP_LIMIT)
            hidden[2 * h + e] = ((up + 1.0) * gate * jax.nn.sigmoid(GLU_ALPHA * gate)).astype(
                BF16
            )

    goals = [ring(z, far)]
    for hop in range(1, far):
        goals += [ring(z, far - hop), ring(z, hop - far)]
    goals += [z]

    def goal_of(way, hop):
        return 0 if hop == 0 else 2 * hop - 1 + way

    def down(g):
        wide = pl.ds(pl.multiple_of(goals[g] * 256, 256), 256)
        for he in range(4):
            y = nn_dot(hidden[he], down_w[he % 2, :, wide]).astype(BF16)
            ybuf[0, g, he] = y[:, :128]
            ybuf[1, g, he] = y[:, 128:]
        y_copy(g).start()

    def y_copy(g):
        return remote(
            ybuf.at[1 - c, g], prec.at[g], y_send.at[0], y_recv.at[g], ep, partner
        )

    def sum_copy(way, hop, he):
        to = ring(z, 1) if way == 0 else ring(z, -1)
        at = (way * far + hop) * 4 + he
        return remote(
            rsend.at[at], rrecv.at[at], r_send.at[0], r_recv.at[at], ep, 2 * to + c
        )

    def own_sum(g, he):
        return ybuf[c, g, he].astype(F32) + prec[g, he].astype(F32)

    def arrived_sum(total, way, hop, he):
        if hop > 0 or he // 2 == way:
            sum_copy(way, hop, he).wait_recv()
            total = total + rrecv[(way * far + hop) * 4 + he].astype(F32)
        return total

    down(0)
    for g in (1, 2):
        if far > 1:
            down(g)
    y_copy(0).wait_recv()
    for way in range(2):
        for e in range(2):
            he = 2 * way + e
            rsend[way * far * 4 + he] = own_sum(0, he).astype(BF16)
            sum_copy(way, 0, he).start()
    spread(2)

    def pair(a, places, m, cond):
        def work():
            @pl.when(cond)
            def _():
                attend([held_at(a, b) for b in places], (m,))

        return work

    def own_row(m):
        def work():
            @pl.when(px >= 2)
            def _():
                attend([held_at(0, -1), held_at(0, -2)], (m,))

            @pl.when(px == 1)
            def _():
                attend([held_at(0, -1)], (m,))

        return work

    def own_third():
        @pl.when(px == 3)
        def _():
            attend([held_at(0, -3)], (0, 1))

    up_1, up_2, up_3 = py >= 1, py >= 2, py >= 3
    fillers = [
        own_row(0),
        own_row(1),
        pair(-1, (0, 1), 0, up_1),
        pair(-1, (0, 1), 1, up_1),
        pair(-3, (0, 1), 0, up_3),
        pair(-3, (0, 1), 1, up_3),
        own_third,
        lambda: spread(3),
        pair(-1, (-1, 2), 0, up_1),
        pair(-1, (-1, 2), 1, up_1),
        pair(-3, (-1, 2), 0, up_3),
        pair(-3, (-1, 2), 1, up_3),
        pair(-2, (0, 1), 0, up_2),
        pair(-2, (0, 1), 1, up_2),
        lambda: spread(4),
        pair(-2, (-1, 2), 0, up_2),
        pair(-2, (-1, 2), 1, up_2),
    ]

    def fill(count=1):
        for _ in range(count):
            if fillers:
                fillers.pop(0)()

    for hop in range(1, far):
        for way in range(2):
            y_copy(goal_of(way, hop)).wait_recv()
        for he in range(4):
            fill()
            for way in range(2):
                part_at = he if way == 0 else (he + 2) % 4
                total = arrived_sum(own_sum(goal_of(way, hop), part_at), way, hop - 1, part_at)
                rsend[(way * far + hop) * 4 + part_at] = total.astype(BF16)
                sum_copy(way, hop, part_at).start()
            if he == 1:
                for way in range(2):
                    if hop < far - 1:
                        down(goal_of(way, hop + 1))
                    elif way == 0:
                        down(n_z - 1)
    if far == 1:
        down(n_z - 1)

    last = n_z - 1
    y_copy(last).wait_recv()
    for h in range(2):
        totals = []
        for e in range(2):
            he = 2 * h + e
            fill(2)
            total = own_sum(last, he)
            for way in range(2):
                total = arrived_sum(total, way, far - 1, he)
            totals.append(total.reshape(sources_half, 1, cap, 128))
        back_send[h * half : (h + 1) * half] = (
            jnp.concatenate(totals, axis=1).reshape(half, 128).astype(BF16)
        )
        for s in range(h * sources_half, (h + 1) * sources_half):

            @pl.when(ep != s)
            def _(s=s):
                remote(
                    back_send.at[pl.ds(s * block, block)],
                    back.at[mine],
                    b_sem.at[0],
                    b_sem.at[1],
                    s,
                    tp,
                ).start()

    back[mine, :] = back_send[mine, :]
    fill(len(fillers))

    mix = mix_ref[...]
    for r in range(0, q_rows, tile):
        one, two = pl.ds(r, tile), pl.ds(q_rows + r, tile)
        blend = acc[one, :width] / acc[one, width:] - mix * (acc[two, :width] / acc[two, width:])
        mean = jnp.mean(blend * blend, axis=1, keepdims=True)
        scaled = blend * lax.rsqrt(mean + SUB_EPS)
        attn_ref[one, :] = (scaled * sub_gain_ref[...] * OUT_SCALE).astype(BF16)
    attn_out = pltpu.make_async_copy(attn_ref, attn_hbm, out_sem.at[0])
    attn_out.start()

    remote(arrived, arrived, d_sem.at[0], d_sem.at[1], ep, partner).wait_send()
    for n, buf in enumerate((kbuf, vbuf)):
        whole = buf.at[pl.ds(0, n_ep - 1)]
        remote(whole, whole, kv_send.at[n], kv_recv.at[n, 0], ep, partner).wait_send()
    whole = gathered.at[pl.ds(0, n_z - 1)]
    remote(whole, whole, g_send.at[0], g_recv.at[0], ep, partner).wait_send()
    whole = gathered.at[pl.ds(0, n_z)]
    remote(whole, whole, p_send.at[0], p_recv.at[0], ep, partner).wait_send()
    remote(ybuf.at[0], prec, y_send.at[0], y_recv.at[0], ep, partner).wait_send()
    sent = pl.ds(0, 4 * (n_z - 1))
    remote(rsend.at[sent], rrecv.at[sent], r_send.at[0], r_recv.at[0], ep, partner).wait_send()
    weight = jnp.concatenate(
        [pick_weight_ref[...], jnp.zeros((126, rows), F32)], axis=0
    ).T

    piece = back.at[pl.ds(0, others)]
    remote(piece, piece, b_sem.at[0], b_sem.at[1], ep, partner).wait()
    result = back[...]
    moe_ref[...] = (
        tn_dot(picks[0], result) * weight[:, 0:1] + tn_dot(picks[1], result) * weight[:, 1:2]
    ).astype(BF16)
    moe_out = pltpu.make_async_copy(moe_ref, moe_hbm, out_sem.at[1])
    moe_out.start()
    attn_out.wait()
    moe_out.wait()


def shards(
    queries,
    keys,
    values,
    mix_weight,
    sub_gain,
    tokens,
    routes,
    route_weights,
    expert_gain,
    gate_weight,
    up_weight,
    down_weight,
):
    n_ep, n_tp = lax.axis_size("ep"), lax.axis_size("tp")
    n_z = n_tp // 2
    rows, pick_count = routes.shape
    experts = n_ep * gate_weight.shape[0]
    cap = 3 * rows * pick_count // (2 * experts)
    slots = experts * cap
    part = slots // 4
    q_rows, _, qk_width = queries.shape
    v_width = values.shape[2]
    width = expert_gain.shape[0]
    ff = gate_weight.shape[2]
    cfg = dict(n_ep=n_ep, n_tp=n_tp, cap=cap, rows=rows, width=width)
    dma = pltpu.SemaphoreType.DMA
    vmem = pltpu.VMEM
    anywhere = pl.BlockSpec(memory_space=pl.ANY)
    attn_out, moe_out = pl.pallas_call(
        functools.partial(kernel, cfg),
        name="layer",
        out_shape=(
            jax.ShapeDtypeStruct((q_rows, v_width), BF16),
            jax.ShapeDtypeStruct((rows, tokens.shape[1]), BF16),
        ),
        in_specs=[anywhere] * 12,
        out_specs=(anywhere, anywhere),
        scratch_shapes=[
            vmem((q_rows, qk_width), BF16),
            vmem((1, 1), F32),
            vmem((1, v_width), F32),
            vmem(tokens.shape, BF16),
            vmem((pick_count, rows), jnp.int32),
            vmem((pick_count, rows), F32),
            vmem((n_z, 1, width // n_z), F32),
            vmem(gate_weight.shape, BF16),
            vmem(up_weight.shape, BF16),
            vmem(down_weight.shape, BF16),
            vmem((q_rows, v_width), BF16),
            vmem((rows, tokens.shape[1]), BF16),
            vmem((2 * q_rows, qk_width), BF16),
            vmem((n_ep, q_rows, qk_width), BF16),
            vmem((n_ep, q_rows, v_width), BF16),
            vmem((2 * q_rows, 2 * v_width), F32),
            vmem((2 * q_rows, 128), F32),
            vmem((2, slots, rows), BF16),
            vmem((slots, tokens.shape[1]), BF16),
            vmem((n_tp, slots, tokens.shape[1]), BF16),
            vmem((2, 2, 2, part, ff), F32),
            vmem((2, slots // 2, 128), F32),
            vmem((4, part, ff), BF16),
            vmem((2, n_z, 4, part, 128), BF16),
            vmem((n_z, 4, part, 128), BF16),
            vmem((4 * n_z, part, 128), BF16),
            vmem((4 * n_z, part, 128), BF16),
            vmem((slots, 128), BF16),
            vmem((slots, 128), BF16),
            dma((12,)),
            dma((2,)),
            dma((2,)),
            dma((2, n_ep)),
            dma((2,)),
            dma((1,)),
            dma((4 * n_z,)),
            dma((1,)),
            dma((2 * n_z,)),
            dma((1,)),
            dma((n_z,)),
            dma((1,)),
            dma((4 * n_z,)),
            dma((2,)),
        ],
        compiler_params=pltpu.CompilerParams(
            collective_id=0, has_side_effects=True, vmem_limit_bytes=60 * 1024 * 1024
        ),
    )(
        queries.reshape(q_rows, qk_width),
        keys.reshape(q_rows, qk_width),
        values.reshape(q_rows, v_width),
        mix_weight.reshape(1, 1),
        sub_gain.reshape(1, v_width),
        tokens,
        routes.T,
        route_weights.T,
        expert_gain.reshape(n_z, 1, width // n_z),
        gate_weight,
        up_weight,
        down_weight,
    )
    return attn_out.reshape(q_rows, 1, v_width), moe_out


def solution(mesh):
    return jax.shard_map(
        shards,
        mesh=mesh,
        in_specs=(
            P("ep", "tp", None),
            P("ep", "tp", None),
            P("ep", "tp", None),
            P("tp"),
            P(),
            P("ep", "tp"),
            P("ep", None),
            P("ep", None),
            P(),
            P("ep", None, "tp"),
            P("ep", None, "tp"),
            P("ep", "tp", None),
        ),
        out_specs=(P("ep", "tp", None), P("ep", "tp")),
        check_vma=False,
    )
```

time: 121 us -> 70.2 us (0.58); the launches traced: 119 us -> 70 us
  Pallas kernels: 112 us -> 65.7 us
  local copies, waits for them, and re-layouts: 5.78 us -> 3.04 us
    pallas_call x1, Pallas kernels: 112 us -> 65.7 us  [shards(): pl.pallas_call(functools.partial(kernel, cfg), name='layer', out_shape=(j...]
    unnamed x4 -> x2, local copies, waits for them, and re-layouts: 5.78 us -> 3.04 us
where the time goes in v2:
time: 70.2 us; the launch traced here: 70 us
  Pallas kernels  65.7 us (94%)
  local copies, waits for them, and re-layouts  3.04 us (4%)
  between operations  1.29 us (2%)
    pallas_call x1, Pallas kernels, shards(): pl.pallas_call(functools.partial(kernel, cfg), name='layer', out_shape=(j...  65.7 us
    unnamed x2, local copies, waits for them, and re-layouts  3.04 us

profile of v2, /device:TPU:1, one launch (start us, length us, event | category | flops | bytes accessed | tf_op | source)
XLA Modules:
  0.0 70.0 jit_solution(11807154780722413143)
XLA Ops:
  1.3 65.7 %layer.1 = (bf16[512,128]{1,0:T(8,128)(2,1)}, bf16[256,128]{1,0:T(8,128)(2,1)}) custom-call(bf16[512,128]{1,0:T(8,128)(2,1)} %bitcast.10, bf16[512,128]{1,0:T(8,128)(2,1)} %bitcast.11, bf16[512,128]{1,0:T(8,128)(2,1)} %bitcast.12, f32[1,1]{1,0:T(1,128)} %bitcast.9.mix_hbm, f32[1,128]{1,0:T(1,128)} %bitcast.17, bf16[256,128]{1,0:T(8,128)(2,1)} %tokens_hbm.1, ...), custom_call_target="tpu_custom_call" | custom-call | tf_op jit(solution)/shard_map/layer/pallas_call | solution.py:601
  67.0 1.6 %copy.17 = bf16[512,1,128]{2,0,1:T(8,128)(2,1)} copy(bf16[512,1,128]{2,0,1:T(8,128)(2,1)} %bitcast.13) | data formatting | bytes 262144
  68.6 1.5 %copy.18 = bf16[256,128]{1,0:T(8,128)(2,1)} copy(bf16[256,128]{1,0:T(8,128)(2,1)} %get-tuple-element.9) | data formatting | bytes 131072

commit v3 on v2

--- a/solution.py
+++ b/solution.py
@@ -21,10 +21,6 @@
 
 def nt_dot(a, b):
     return lax.dot_general(a, b, (((1,), (1,)), ((), ())), preferred_element_type=F32)
-
-
-def tn_dot(a, b):
-    return lax.dot_general(a, b, (((0,), (0,)), ((), ())), preferred_element_type=F32)
 
 
 def nn_dot(a, b):
@@ -194,8 +190,6 @@
     slot_at = lax.broadcasted_iota(jnp.int32, (slots, rows), 0).astype(F32)
     pick_0 = (slot_at == jnp.broadcast_to(target[:, :rows], (slots, rows))).astype(F32)
     pick_1 = (slot_at == jnp.broadcast_to(target[:, rows:], (slots, rows))).astype(F32)
-    picks[0] = pick_0.astype(BF16)
-    picks[1] = pick_1.astype(BF16)
     out_rows = nn_dot((pick_0 + pick_1).astype(BF16), tokens_ref[...]).astype(BF16)
     outgoing[...] = out_rows
     mine = pl.ds(pl.multiple_of(ep * block, block), block)
@@ -286,8 +280,13 @@
     for copy in loads[3:5]:
         copy.wait()
     attend((0,), first=True)
-    spread(0)
-
+
+    column = jnp.broadcast_to(target, (128, pairs)).T
+    slot_on = lax.broadcasted_iota(jnp.int32, (rows, 128), 1).astype(F32)
+    for n in range(2):
+        at_row = column[n * rows : (n + 1) * rows]
+        for s0 in range(0, slots, 128):
+            picks[n, :, s0 : s0 + 128] = (slot_on + float(s0) == at_row).astype(F32).astype(BF16)
     arrived = gathered.at[tp, pl.ds(0, others)]
     remote(arrived, arrived, d_sem.at[0], d_sem.at[1], ep, partner).wait_recv()
 
@@ -348,11 +347,52 @@
                 product = nn_dot(rows_e, w[e, deep, :])
                 pre[h, e, n] = product if hop == 0 else pre[h, e, n] + product
 
+    spread(0)
     for copy in loads[5:]:
         copy.wait()
-    spread(1)
+    for h in range(2):
+        expert_in(0, 0, h)
+
+    y_1, y_2, y_3 = py >= 1, py >= 2, py >= 3
+    x_1, x_2, x_3 = px >= 1, px >= 2, px >= 3
+
+    def pieces(*cases):
+        def work(m):
+            taken = None
+            for cond, places in cases:
+                now = cond if taken is None else jnp.logical_and(cond, jnp.logical_not(taken))
+
+                @pl.when(now)
+                def _(places=places):
+                    attend([held_at(a, b) for a, b in places], (m,))
+
+                taken = cond if taken is None else jnp.logical_or(taken, cond)
+
+        return [functools.partial(work, 0), functools.partial(work, 1)]
+
+    both_2 = jnp.logical_and(x_2, y_2)
+    fillers = [
+        *pieces((y_3, ((-1, 0), (1, 0))), (y_1, ((-1, 0),))),
+        *pieces((x_3, ((0, -1), (0, 1))), (x_1, ((0, -1),))),
+        lambda: spread(2),
+        *pieces((y_1, ((-1, -1), (-1, 1)))),
+        *pieces((y_3, ((1, -1), (1, 1)))),
+        *pieces((both_2, ((0, 2), (2, 0))), (x_2, ((0, 2),)), (y_2, ((2, 0),))),
+        lambda: spread(3),
+        *pieces((y_3, ((-1, 2), (1, 2))), (y_1, ((-1, 2),))),
+        *pieces((y_2, ((2, -1), (2, 1)))),
+        lambda: spread(4),
+        *pieces((y_2, ((2, 2),))),
+    ]
+
+    def fill(count=1):
+        for _ in range(count):
+            if fillers:
+                fillers.pop(0)()
 
     for hop in range(1, far + 1):
+        if hop == min(2, far):
+            spread(1)
         for step in range(4 if hop < far else 2):
             for way in range(2):
                 sub = step if hop < far else 2 * way + step
@@ -362,14 +402,15 @@
             if step % 2 == 1:
                 h = step // 2
                 for way in range(2):
-                    if hop < far:
-                        partner_copy(way, hop, h, c).start()
-                    else:
-                        partner_copy(way, hop, way, c).start()
-                for half_at in (h,) if hop < far else (0, 1):
-                    expert_in(0, hop - 1, half_at)
-                    if hop > 1:
-                        expert_in(1, hop - 1, half_at)
+                    partner_copy(way, hop, h if hop < far else way, c).start()
+            if step == 0 and hop > 1:
+                for way in range(2):
+                    expert_in(way, hop - 1, 1)
+            if step == 2:
+                for way in range(2):
+                    expert_in(way, hop, 0)
+            if hop in (2, 3) and step % 2 == 1:
+                fill()
     for way in range(2):
         expert_in(way, far, way)
 
@@ -421,73 +462,23 @@
         return total
 
     down(0)
-    for g in (1, 2):
-        if far > 1:
-            down(g)
     y_copy(0).wait_recv()
     for way in range(2):
         for e in range(2):
             he = 2 * way + e
             rsend[way * far * 4 + he] = own_sum(0, he).astype(BF16)
             sum_copy(way, 0, he).start()
-    spread(2)
-
-    def pair(a, places, m, cond):
-        def work():
-            @pl.when(cond)
-            def _():
-                attend([held_at(a, b) for b in places], (m,))
-
-        return work
-
-    def own_row(m):
-        def work():
-            @pl.when(px >= 2)
-            def _():
-                attend([held_at(0, -1), held_at(0, -2)], (m,))
-
-            @pl.when(px == 1)
-            def _():
-                attend([held_at(0, -1)], (m,))
-
-        return work
-
-    def own_third():
-        @pl.when(px == 3)
-        def _():
-            attend([held_at(0, -3)], (0, 1))
-
-    up_1, up_2, up_3 = py >= 1, py >= 2, py >= 3
-    fillers = [
-        own_row(0),
-        own_row(1),
-        pair(-1, (0, 1), 0, up_1),
-        pair(-1, (0, 1), 1, up_1),
-        pair(-3, (0, 1), 0, up_3),
-        pair(-3, (0, 1), 1, up_3),
-        own_third,
-        lambda: spread(3),
-        pair(-1, (-1, 2), 0, up_1),
-        pair(-1, (-1, 2), 1, up_1),
-        pair(-3, (-1, 2), 0, up_3),
-        pair(-3, (-1, 2), 1, up_3),
-        pair(-2, (0, 1), 0, up_2),
-        pair(-2, (0, 1), 1, up_2),
-        lambda: spread(4),
-        pair(-2, (-1, 2), 0, up_2),
-        pair(-2, (-1, 2), 1, up_2),
-    ]
-
-    def fill(count=1):
-        for _ in range(count):
-            if fillers:
-                fillers.pop(0)()
+    for g in (1, 2):
+        if far > 1:
+            down(g)
+    fill()
 
     for hop in range(1, far):
         for way in range(2):
             y_copy(goal_of(way, hop)).wait_recv()
         for he in range(4):
-            fill()
+            if hop > 1 or he > 0:
+                fill()
             for way in range(2):
                 part_at = he if way == 0 else (he + 2) % 4
                 total = arrived_sum(own_sum(goal_of(way, hop), part_at), way, hop - 1, part_at)
@@ -561,12 +552,17 @@
     remote(piece, piece, b_sem.at[0], b_sem.at[1], ep, partner).wait()
     result = back[...]
     moe_ref[...] = (
-        tn_dot(picks[0], result) * weight[:, 0:1] + tn_dot(picks[1], result) * weight[:, 1:2]
+        nn_dot(picks[0], result) * weight[:, 0:1] + nn_dot(picks[1], result) * weight[:, 1:2]
     ).astype(BF16)
     moe_out = pltpu.make_async_copy(moe_ref, moe_hbm, out_sem.at[1])
     moe_out.start()
     attn_out.wait()
     moe_out.wait()
+
+
+def hand_on(attn_in, moe_in, attn_ref, moe_ref):
+    attn_ref[...] = attn_in[...]
+    moe_ref[...] = moe_in[...]
 
 
 def shards(
@@ -625,7 +621,7 @@
             vmem((n_ep, q_rows, v_width), BF16),
             vmem((2 * q_rows, 2 * v_width), F32),
             vmem((2 * q_rows, 128), F32),
-            vmem((2, slots, rows), BF16),
+            vmem((2, rows, slots), BF16),
             vmem((slots, tokens.shape[1]), BF16),
             vmem((n_tp, slots, tokens.shape[1]), BF16),
             vmem((2, 2, 2, part, ff), F32),
@@ -669,6 +665,17 @@
         up_weight,
         down_weight,
     )
+    whole = pl.BlockSpec(memory_space=vmem)
+    attn_out, moe_out = pl.pallas_call(
+        hand_on,
+        name="hand_on",
+        out_shape=(
+            jax.ShapeDtypeStruct(attn_out.shape, BF16),
+            jax.ShapeDtypeStruct(moe_out.shape, BF16),
+        ),
+        in_specs=[whole] * 2,
+        out_specs=(whole, whole),
+    )(attn_out, moe_out)
     return attn_out.reshape(q_rows, 1, v_width), moe_out
 
 

time: 70.2 us -> 66.2 us (0.943)
  local copies, waits for them, and re-layouts: 3.04 us -> 0 us
  Pallas kernels: 65.7 us -> 64.3 us
    unnamed x2 -> x0, local copies, waits for them, and re-layouts: 3.04 us -> none
    pallas_call x1, Pallas kernels: 65.7 us -> 62.7 us  [shards(): pl.pallas_call(functools.partial(kernel, cfg), name='layer', out_shape=(j...]
    pallas_call x0 -> x1, Pallas kernels: none -> 1.59 us  [shards(): pl.pallas_call(hand_on, name='hand_on', out_shape=(jax.ShapeDtypeStruct(a...]
where the time goes in v3:
time: 66.2 us; the launch traced here: 65.6 us
  Pallas kernels  64.3 us (97%)
  between operations  1.29 us (2%)
    pallas_call x1, Pallas kernels, shards(): pl.pallas_call(functools.partial(kernel, cfg), name='layer', out_shape=(j...  62.7 us
    pallas_call x1, Pallas kernels, shards(): pl.pallas_call(hand_on, name='hand_on', out_shape=(jax.ShapeDtypeStruct(a...  1.59 us

profile of v3, /device:TPU:1, one launch (start us, length us, event | category | flops | bytes accessed | tf_op | source)
XLA Modules:
  0.0 65.6 jit_solution(16619234467094148422)
XLA Ops:
  1.3 62.7 %layer.1 = (bf16[512,128]{1,0:T(8,128)(2,1)}, bf16[256,128]{1,0:T(8,128)(2,1)}) custom-call(bf16[512,128]{1,0:T(8,128)(2,1)} %bitcast.10, bf16[512,128]{1,0:T(8,128)(2,1)} %bitcast.11, bf16[512,128]{1,0:T(8,128)(2,1)} %bitcast.12, f32[1,1]{1,0:T(1,128)} %bitcast.9.mix_hbm, f32[1,128]{1,0:T(1,128)} %bitcast.16, bf16[256,128]{1,0:T(8,128)(2,1)} %tokens_hbm.1, ...), custom_call_target="tpu_custom_call" | custom-call | tf_op jit(solution)/shard_map/layer/pallas_call | solution.py:597
  64.0 1.6 %hand_on.1 = (bf16[512,128]{1,0:T(8,128)(2,1)}, bf16[256,128]{1,0:T(8,128)(2,1)}) custom-call(bf16[512,128]{1,0:T(8,128)(2,1)} %get-tuple-element.6.attn_in, bf16[256,128]{1,0:T(8,128)(2,1)} %get-tuple-element.7.moe_in), custom_call_target="tpu_custom_call" | custom-call | tf_op jit(solution)/shard_map/hand_on/pallas_call | solution.py:669

commit v4 on v3

--- a/solution.py
+++ b/solution.py
@@ -50,6 +50,8 @@
 STEP = {"x+": (0, 1), "x-": (0, -1), "y+": (1, 0), "y-": (-1, 0)}
 MIRROR = {"x+": "y-", "x-": "y+", "y+": "x-", "y-": "x+"}
 SIDE = 4
+ROW_ORDER = (0, 1, -1, 2)
+FAR_FIRST = tuple(sorted(((a, b) for a in range(4) for b in range(4)), key=lambda p: -min(p[0], 4 - p[0]) - min(p[1], 4 - p[1])))[:-1]
 
 
 def kernel(
@@ -101,7 +103,8 @@
     out_sem,
     kv_send,
     kv_recv,
-    d_sem,
+    d_send,
+    d_recv,
     g_send,
     g_recv,
     p_send,
@@ -140,10 +143,11 @@
         )
 
     barrier = pltpu.get_barrier_semaphore()
-    for off in range(1, n_ep):
-        pl.semaphore_signal(
-            barrier, inc=1, device_id=(lax.rem(ep + off, n_ep), tp), device_id_type=MESH
-        )
+    def across(dy, dx):
+        return lax.rem(py + dy + SIDE, SIDE) * SIDE + lax.rem(px + dx + SIDE, SIDE)
+
+    for dy, dx in FAR_FIRST:
+        pl.semaphore_signal(barrier, inc=1, device_id=(across(dy, dx), tp), device_id_type=MESH)
     for to in (2 * ring(z, 1) + c, 2 * ring(z, -1) + c, partner):
         pl.semaphore_signal(barrier, inc=1, device_id=(ep, to), device_id_type=MESH)
 
@@ -193,7 +197,8 @@
     out_rows = nn_dot((pick_0 + pick_1).astype(BF16), tokens_ref[...]).astype(BF16)
     outgoing[...] = out_rows
     mine = pl.ds(pl.multiple_of(ep * block, block), block)
-    gathered[tp, mine, :] = outgoing[mine, :]
+    own = pl.ds(pl.multiple_of(px * block, block), block)
+    gathered[tp, own, :] = outgoing[mine, :]
 
     loads[2].wait()
     q_all = q_ref[...]
@@ -205,16 +210,20 @@
 
     pl.semaphore_wait(barrier, n_ep - 1 + 3)
 
-    for off in range(1, n_ep):
-        to = lax.rem(ep + off, n_ep)
-        remote(
-            outgoing.at[pl.ds(pl.multiple_of(to * block, block), block)],
-            gathered.at[tp, mine],
-            d_sem.at[0],
-            d_sem.at[1],
-            to,
-            tp,
-        ).start()
+    for group, dy in enumerate(ROW_ORDER):
+        for dx in range(SIDE):
+            if dy == 0 and dx == 0:
+                continue
+            to = across(-dy, dx)
+            at = pl.multiple_of((group * SIDE + px) * block, block)
+            remote(
+                outgoing.at[pl.ds(pl.multiple_of(to * block, block), block)],
+                gathered.at[tp, pl.ds(at, block)],
+                d_send.at[0],
+                d_recv.at[group],
+                to,
+                tp,
+            ).start()
     others = (n_ep - 1) * block
 
     exponent = (q_ref.shape[1] // 2) ** (-0.5) * math.log2(math.e)
@@ -243,7 +252,10 @@
             olds = [row_max[pl.ds(r, tile), :] for r in at]
             tops = [jnp.maximum(o, t) for o, t in zip(olds, tops)]
         weights = [
-            jnp.exp2((s - t[:, :1]) * exponent).astype(BF16) for s, t in zip(scores, tops)
+            jnp.exp2((s - jnp.concatenate([t] * (s.shape[1] // 128), axis=1)) * exponent).astype(
+                BF16
+            )
+            for s, t in zip(scores, tops)
         ]
         for i, r in enumerate(at):
             where = pl.ds(r, tile)
@@ -260,21 +272,18 @@
 
     def spread(stage):
         waits, sends = STAGES[stage]
-        for n, buf in enumerate((kbuf, vbuf)):
-            for a, b in waits:
-                at = held_at(a, b) if n == 0 else held_at(-b, -a)
-                remote(
-                    buf.at[at], buf.at[at], kv_send.at[n], kv_recv.at[n, at], ep, partner
-                ).wait_recv()
+        if waits:
+            all_of = kbuf.at[pl.ds(0, 2 * len(waits))]
+            remote(all_of, all_of, kv_send.at[0], kv_recv.at[stage - 1], ep, partner).wait_recv()
         for (a, b), way in sends:
             for n, buf in enumerate((kbuf, vbuf)):
                 if n == 1:
                     a, b, way = -b, -a, MIRROR[way]
                 dy, dx = STEP[way]
-                to = lax.rem(py + dy + SIDE, SIDE) * SIDE + lax.rem(px + dx + SIDE, SIDE)
+                to = across(dy, dx)
                 at = held_at(a - dy, b - dx)
                 remote(
-                    buf.at[held_at(a, b)], buf.at[at], kv_send.at[n], kv_recv.at[n, at], to, tp
+                    buf.at[held_at(a, b)], buf.at[at], kv_send.at[n], kv_recv.at[stage], to, tp
                 ).start()
 
     for copy in loads[3:5]:
@@ -287,9 +296,6 @@
         at_row = column[n * rows : (n + 1) * rows]
         for s0 in range(0, slots, 128):
             picks[n, :, s0 : s0 + 128] = (slot_on + float(s0) == at_row).astype(F32).astype(BF16)
-    arrived = gathered.at[tp, pl.ds(0, others)]
-    remote(arrived, arrived, d_sem.at[0], d_sem.at[1], ep, partner).wait_recv()
-
     cut = half // 2
 
     def source_of(way, hop):
@@ -319,11 +325,13 @@
         )
 
     for sub in range(4):
+        group = gathered.at[tp, pl.ds(0, (SIDE - 1 if sub == 0 else SIDE) * block)]
+        remote(group, group, d_send.at[0], d_recv.at[sub], ep, partner).wait_recv()
         for way in range(2):
             if sub in subs_of(way, 0):
                 gather_copy(way, 0, sub).start()
-    for h in range(2):
-        partner_copy(0, 0, h, c).start()
+        if sub % 2 == 1:
+            partner_copy(0, 0, sub // 2, c).start()
 
     def by_expert(value):
         w = value.shape[1]
@@ -381,9 +389,8 @@
         lambda: spread(3),
         *pieces((y_3, ((-1, 2), (1, 2))), (y_1, ((-1, 2),))),
         *pieces((y_2, ((2, -1), (2, 1)))),
-        lambda: spread(4),
-        *pieces((y_2, ((2, 2),))),
     ]
+    last_fillers = [lambda: spread(4), *pieces((y_2, ((2, 2),)))]
 
     def fill(count=1):
         for _ in range(count):
@@ -391,9 +398,9 @@
                 fillers.pop(0)()
 
     for hop in range(1, far + 1):
-        if hop == min(2, far):
-            spread(1)
         for step in range(4 if hop < far else 2):
+            if (hop, step) == (2, 2):
+                spread(1)
             for way in range(2):
                 sub = step if hop < far else 2 * way + step
                 gather_wait(way, hop, sub)
@@ -409,12 +416,9 @@
             if step == 2:
                 for way in range(2):
                     expert_in(way, hop, 0)
-            if hop in (2, 3) and step % 2 == 1:
+            if (hop, step) in ((2, 2), (2, 3), (3, 1), (3, 3)):
                 fill()
-    for way in range(2):
-        expert_in(way, far, way)
-
-    for h in range(2):
+    def activate(h):
         factor = lax.rsqrt(squares[h] / float(cfg["width"]) + NORM_EPS)
         for e, f in enumerate(by_expert(factor)):
             f = jnp.concatenate([f, f], axis=1)
@@ -432,17 +436,20 @@
     def goal_of(way, hop):
         return 0 if hop == 0 else 2 * hop - 1 + way
 
-    def down(g):
+    def down(g, halves=(0, 1)):
         wide = pl.ds(pl.multiple_of(goals[g] * 256, 256), 256)
-        for he in range(4):
-            y = nn_dot(hidden[he], down_w[he % 2, :, wide]).astype(BF16)
-            ybuf[0, g, he] = y[:, :128]
-            ybuf[1, g, he] = y[:, 128:]
-        y_copy(g).start()
-
-    def y_copy(g):
+        for h in halves:
+            for e in range(2):
+                y = nn_dot(hidden[2 * h + e], down_w[e, :, wide]).astype(BF16)
+                ybuf[0, g, 2 * h + e] = y[:, :128]
+                ybuf[1, g, 2 * h + e] = y[:, 128:]
+        y_copy(g, halves).start()
+
+    def y_copy(g, halves=(0, 1)):
+        at = pl.ds(2 * halves[0], 2 * len(halves))
+        sem = g if halves[0] == 0 else n_z
         return remote(
-            ybuf.at[1 - c, g], prec.at[g], y_send.at[0], y_recv.at[g], ep, partner
+            ybuf.at[1 - c, g, at], prec.at[g, at], y_send.at[0], y_recv.at[sem], ep, partner
         )
 
     def sum_copy(way, hop, he):
@@ -461,9 +468,12 @@
             total = total + rrecv[(way * far + hop) * 4 + he].astype(F32)
         return total
 
-    down(0)
-    y_copy(0).wait_recv()
+    for h in range(2):
+        expert_in(h, far, h)
+        activate(h)
+        down(0, (h,))
     for way in range(2):
+        y_copy(0, (way,)).wait_recv()
         for e in range(2):
             he = 2 * way + e
             rsend[way * far * 4 + he] = own_sum(0, he).astype(BF16)
@@ -471,8 +481,6 @@
     for g in (1, 2):
         if far > 1:
             down(g)
-    fill()
-
     for hop in range(1, far):
         for way in range(2):
             y_copy(goal_of(way, hop)).wait_recv()
@@ -480,7 +488,7 @@
             if hop > 1 or he > 0:
                 fill()
             for way in range(2):
-                part_at = he if way == 0 else (he + 2) % 4
+                part_at = (he + 2) % 4 if way == 0 else he
                 total = arrived_sum(own_sum(goal_of(way, hop), part_at), way, hop - 1, part_at)
                 rsend[(way * far + hop) * 4 + part_at] = total.astype(BF16)
                 sum_copy(way, hop, part_at).start()
@@ -499,7 +507,7 @@
         totals = []
         for e in range(2):
             he = 2 * h + e
-            fill(2)
+            fill()
             total = own_sum(last, he)
             for way in range(2):
                 total = arrived_sum(total, way, far - 1, he)
@@ -507,20 +515,22 @@
         back_send[h * half : (h + 1) * half] = (
             jnp.concatenate(totals, axis=1).reshape(half, 128).astype(BF16)
         )
-        for s in range(h * sources_half, (h + 1) * sources_half):
-
-            @pl.when(ep != s)
-            def _(s=s):
+        for p in range(h * sources_half, (h + 1) * sources_half):
+
+            @pl.when(px != p)
+            def _(p=p):
+                to = lax.rem(py + ROW_ORDER[p // SIDE] + SIDE, SIDE) * SIDE + p % SIDE
                 remote(
-                    back_send.at[pl.ds(s * block, block)],
+                    back_send.at[pl.ds(p * block, block)],
                     back.at[mine],
                     b_sem.at[0],
                     b_sem.at[1],
-                    s,
+                    to,
                     tp,
                 ).start()
 
-    back[mine, :] = back_send[mine, :]
+    back[mine, :] = back_send[own, :]
+    fillers += last_fillers
     fill(len(fillers))
 
     mix = mix_ref[...]
@@ -533,10 +543,11 @@
     attn_out = pltpu.make_async_copy(attn_ref, attn_hbm, out_sem.at[0])
     attn_out.start()
 
-    remote(arrived, arrived, d_sem.at[0], d_sem.at[1], ep, partner).wait_send()
+    sent = outgoing.at[pl.ds(0, others)]
+    remote(sent, sent, d_send.at[0], d_recv.at[0], ep, partner).wait_send()
     for n, buf in enumerate((kbuf, vbuf)):
         whole = buf.at[pl.ds(0, n_ep - 1)]
-        remote(whole, whole, kv_send.at[n], kv_recv.at[n, 0], ep, partner).wait_send()
+        remote(whole, whole, kv_send.at[n], kv_recv.at[0], ep, partner).wait_send()
     whole = gathered.at[pl.ds(0, n_z - 1)]
     remote(whole, whole, g_send.at[0], g_recv.at[0], ep, partner).wait_send()
     whole = gathered.at[pl.ds(0, n_z)]
@@ -636,14 +647,15 @@
             dma((12,)),
             dma((2,)),
             dma((2,)),
-            dma((2, n_ep)),
-            dma((2,)),
+            dma((len(STAGES) - 1,)),
+            dma((1,)),
+            dma((SIDE,)),
             dma((1,)),
             dma((4 * n_z,)),
             dma((1,)),
             dma((2 * n_z,)),
             dma((1,)),
-            dma((n_z,)),
+            dma((n_z + 1,)),
             dma((1,)),
             dma((4 * n_z,)),
             dma((2,)),

time: 66.2 us -> 62.5 us (0.944)
  Pallas kernels: 64.3 us -> 61.1 us
    pallas_call x1, Pallas kernels: 62.7 us -> 59.5 us  [shards(): pl.pallas_call(functools.partial(kernel, cfg), name='layer', out_shape=(j...]
where the time goes in v4:
time: 62.5 us; the launch traced here: 62.4 us
  Pallas kernels  61.1 us (98%)
  between operations  1.29 us (2%)
    pallas_call x1, Pallas kernels, shards(): pl.pallas_call(functools.partial(kernel, cfg), name='layer', out_shape=(j...  59.5 us
    pallas_call x1, Pallas kernels, shards(): pl.pallas_call(hand_on, name='hand_on', out_shape=(jax.ShapeDtypeStruct(a...  1.59 us

profile of v4, /device:TPU:1, one launch (start us, length us, event | category | flops | bytes accessed | tf_op | source)
XLA Modules:
  0.0 62.4 jit_solution(8834900795768341379)
XLA Ops:
  1.3 59.5 %layer.1 = (bf16[512,128]{1,0:T(8,128)(2,1)}, bf16[256,128]{1,0:T(8,128)(2,1)}) custom-call(bf16[512,128]{1,0:T(8,128)(2,1)} %bitcast.10, bf16[512,128]{1,0:T(8,128)(2,1)} %bitcast.11, bf16[512,128]{1,0:T(8,128)(2,1)} %bitcast.12, f32[1,1]{1,0:T(1,128)} %bitcast.9.mix_hbm, f32[1,128]{1,0:T(1,128)} %bitcast.16, bf16[256,128]{1,0:T(8,128)(2,1)} %tokens_hbm.1, ...), custom_call_target="tpu_custom_call" | custom-call | tf_op jit(solution)/shard_map/layer/pallas_call | solution.py:608
  60.8 1.6 %hand_on.1 = (bf16[512,128]{1,0:T(8,128)(2,1)}, bf16[256,128]{1,0:T(8,128)(2,1)}) custom-call(bf16[512,128]{1,0:T(8,128)(2,1)} %get-tuple-element.6.attn_in, bf16[256,128]{1,0:T(8,128)(2,1)} %get-tuple-element.7.moe_in), custom_call_target="tpu_custom_call" | custom-call | tf_op jit(solution)/shard_map/hand_on/pallas_call | solution.py:681

commit v5 on v4

--- a/solution.py
+++ b/solution.py
@@ -313,7 +313,10 @@
         remote(piece, piece, g_send.at[0], g_recv.at[at], ep, partner).wait_recv()
 
     def subs_of(way, hop):
-        return range(4) if hop < far - 1 else range(2 * way, 2 * way + 2)
+        return range(4) if hop < far - 1 else range(way, 4, 2)
+
+    def sub_at(way, step):
+        return step if way == 0 else step // 2 * 2 + 1 - step % 2
 
     def shard(way, hop):
         return 0 if hop == 0 else (2 * hop - 1 + way if hop < far else n_z - 1)
@@ -327,10 +330,12 @@
     for sub in range(4):
         group = gathered.at[tp, pl.ds(0, (SIDE - 1 if sub == 0 else SIDE) * block)]
         remote(group, group, d_send.at[0], d_recv.at[sub], ep, partner).wait_recv()
-        for way in range(2):
-            if sub in subs_of(way, 0):
-                gather_copy(way, 0, sub).start()
-        if sub % 2 == 1:
+        if sub % 2 == 0:
+            gather_copy(0, 0, sub).start()
+        else:
+            gather_copy(1, 0, sub).start()
+            gather_copy(0, 0, sub).start()
+            gather_copy(1, 0, sub - 1).start()
             partner_copy(0, 0, sub // 2, c).start()
 
     def by_expert(value):
@@ -386,6 +391,8 @@
         *pieces((y_1, ((-1, -1), (-1, 1)))),
         *pieces((y_3, ((1, -1), (1, 1)))),
         *pieces((both_2, ((0, 2), (2, 0))), (x_2, ((0, 2),)), (y_2, ((2, 0),))),
+        lambda: None,
+        lambda: None,
         lambda: spread(3),
         *pieces((y_3, ((-1, 2), (1, 2))), (y_1, ((-1, 2),))),
         *pieces((y_2, ((2, -1), (2, 1)))),
@@ -397,27 +404,6 @@
             if fillers:
                 fillers.pop(0)()
 
-    for hop in range(1, far + 1):
-        for step in range(4 if hop < far else 2):
-            if (hop, step) == (2, 2):
-                spread(1)
-            for way in range(2):
-                sub = step if hop < far else 2 * way + step
-                gather_wait(way, hop, sub)
-                if hop < far and sub in subs_of(way, hop):
-                    gather_copy(way, hop, sub).start()
-            if step % 2 == 1:
-                h = step // 2
-                for way in range(2):
-                    partner_copy(way, hop, h if hop < far else way, c).start()
-            if step == 0 and hop > 1:
-                for way in range(2):
-                    expert_in(way, hop - 1, 1)
-            if step == 2:
-                for way in range(2):
-                    expert_in(way, hop, 0)
-            if (hop, step) in ((2, 2), (2, 3), (3, 1), (3, 3)):
-                fill()
     def activate(h):
         factor = lax.rsqrt(squares[h] / float(cfg["width"]) + NORM_EPS)
         for e, f in enumerate(by_expert(factor)):
@@ -428,6 +414,32 @@
                 BF16
             )
 
+    for hop in range(1, far):
+        for step in range(4):
+            if (hop, step) == (2, 2):
+                spread(1)
+            for way in range(2):
+                sub = sub_at(way, step)
+                gather_wait(way, hop, sub)
+                if sub in subs_of(way, hop):
+                    gather_copy(way, hop, sub).start()
+            if step % 2 == 1:
+                for way in range(2):
+                    partner_copy(way, hop, step // 2, c).start()
+            if step == 0 and hop > 1:
+                for way in range(2):
+                    expert_in(way, hop - 1, 1)
+            if step == 2:
+                for way in range(2):
+                    expert_in(way, hop, 0)
+            if (hop, step) in ((2, 2), (2, 3), (3, 1), (3, 3)):
+                fill()
+
+    def gather_last(h):
+        for way in range(2):
+            gather_wait(way, far, 2 * h + way)
+        partner_copy(0, far, h, c).start()
+
     goals = [ring(z, far)]
     for hop in range(1, far):
         goals += [ring(z, far - hop), ring(z, hop - far)]
@@ -436,20 +448,23 @@
     def goal_of(way, hop):
         return 0 if hop == 0 else 2 * hop - 1 + way
 
-    def down(g, halves=(0, 1)):
+    def down(g, h):
         wide = pl.ds(pl.multiple_of(goals[g] * 256, 256), 256)
-        for h in halves:
-            for e in range(2):
-                y = nn_dot(hidden[2 * h + e], down_w[e, :, wide]).astype(BF16)
-                ybuf[0, g, 2 * h + e] = y[:, :128]
-                ybuf[1, g, 2 * h + e] = y[:, 128:]
-        y_copy(g, halves).start()
-
-    def y_copy(g, halves=(0, 1)):
-        at = pl.ds(2 * halves[0], 2 * len(halves))
-        sem = g if halves[0] == 0 else n_z
+        for e in range(2):
+            y = nn_dot(hidden[2 * h + e], down_w[e, :, wide]).astype(BF16)
+            ybuf[0, g, 2 * h + e] = y[:, :128]
+            ybuf[1, g, 2 * h + e] = y[:, 128:]
+        y_copy(g, h).start()
+
+    def y_copy(g, h):
+        at = pl.ds(2 * h, 2)
         return remote(
-            ybuf.at[1 - c, g, at], prec.at[g, at], y_send.at[0], y_recv.at[sem], ep, partner
+            ybuf.at[1 - c, g, at],
+            prec.at[g, at],
+            y_send.at[0],
+            y_recv.at[2 * g + h],
+            ep,
+            partner,
         )
 
     def sum_copy(way, hop, he):
@@ -463,51 +478,75 @@
         return ybuf[c, g, he].astype(F32) + prec[g, he].astype(F32)
 
     def arrived_sum(total, way, hop, he):
-        if hop > 0 or he // 2 == way:
+        if hop > 0 or he % 2 == way:
             sum_copy(way, hop, he).wait_recv()
             total = total + rrecv[(way * far + hop) * 4 + he].astype(F32)
         return total
 
+    def pass_on(way, hop, he):
+        total = own_sum(goal_of(way, hop), he)
+        if hop > 0:
+            total = arrived_sum(total, way, hop - 1, he)
+        rsend[(way * far + hop) * 4 + he] = total.astype(BF16)
+        sum_copy(way, hop, he).start()
+
+    def begin(h):
+        y_copy(0, h).wait_recv()
+        for way in range(2):
+            pass_on(way, 0, 2 * h + way)
+
+    def fresh(h):
+        for way in range(2):
+            y_copy(goal_of(way, 1), h).wait_recv()
+            pass_on(way, 1, 2 * h + 1 - way)
+
+    def finish_expert(h):
+        expert_in(0, far, h)
+        activate(h)
+        down(0, h)
+
+    gather_last(0)
+    for way in range(2):
+        expert_in(way, far - 1, 1)
+    finish_expert(0)
+    for g in (1, 2):
+        down(g, 0)
+    gather_last(1)
+    begin(0)
+    finish_expert(1)
+    fresh(0)
+    for g in (1, 2):
+        down(g, 1)
+    begin(1)
+    fresh(1)
+    for g in (3, 4):
+        for h in range(2):
+            down(g, h)
+
+    for hop in range(1, far):
+        if hop > 1:
+            for way in range(2):
+                for h in range(2):
+                    y_copy(goal_of(way, hop), h).wait_recv()
+        for step in range(2 if hop == 1 else 0, 4):
+            fill()
+            for way in range(2):
+                e = 1 - way if step < 2 else way
+                pass_on(way, hop, step % 2 * 2 + e)
+            if step == 2:
+                for g in {1: (), 2: (5, 6), 3: (7,)}[hop]:
+                    for h in range(2):
+                        down(g, h)
+
+    last = n_z - 1
     for h in range(2):
-        expert_in(h, far, h)
-        activate(h)
-        down(0, (h,))
-    for way in range(2):
-        y_copy(0, (way,)).wait_recv()
-        for e in range(2):
-            he = 2 * way + e
-            rsend[way * far * 4 + he] = own_sum(0, he).astype(BF16)
-            sum_copy(way, 0, he).start()
-    for g in (1, 2):
-        if far > 1:
-            down(g)
-    for hop in range(1, far):
-        for way in range(2):
-            y_copy(goal_of(way, hop)).wait_recv()
-        for he in range(4):
-            if hop > 1 or he > 0:
-                fill()
-            for way in range(2):
-                part_at = (he + 2) % 4 if way == 0 else he
-                total = arrived_sum(own_sum(goal_of(way, hop), part_at), way, hop - 1, part_at)
-                rsend[(way * far + hop) * 4 + part_at] = total.astype(BF16)
-                sum_copy(way, hop, part_at).start()
-            if he == 1:
-                for way in range(2):
-                    if hop < far - 1:
-                        down(goal_of(way, hop + 1))
-                    elif way == 0:
-                        down(n_z - 1)
-    if far == 1:
-        down(n_z - 1)
-
-    last = n_z - 1
-    y_copy(last).wait_recv()
+        y_copy(last, h).wait_recv()
     for h in range(2):
         totals = []
         for e in range(2):
             he = 2 * h + e
-            fill()
+            if he == 0:
+                fill(3)
             total = own_sum(last, he)
             for way in range(2):
                 total = arrived_sum(total, way, far - 1, he)
@@ -655,7 +694,7 @@
             dma((1,)),
             dma((2 * n_z,)),
             dma((1,)),
-            dma((n_z + 1,)),
+            dma((2 * n_z,)),
             dma((1,)),
             dma((4 * n_z,)),
             dma((2,)),

time: 62.5 us -> 60.5 us (0.968)
  Pallas kernels: 61.1 us -> 58.9 us
    pallas_call x1, Pallas kernels: 59.5 us -> 57.3 us  [shards(): pl.pallas_call(functools.partial(kernel, cfg), name='layer', out_shape=(j...]
where the time goes in v5:
time: 60.5 us; the launch traced here: 60.2 us
  Pallas kernels  58.9 us (97%)
  between operations  1.29 us (2%)
    pallas_call x1, Pallas kernels, shards(): pl.pallas_call(functools.partial(kernel, cfg), name='layer', out_shape=(j...  57.3 us
    pallas_call x1, Pallas kernels, shards(): pl.pallas_call(hand_on, name='hand_on', out_shape=(jax.ShapeDtypeStruct(a...  1.59 us

profile of v5, /device:TPU:1, one launch (start us, length us, event | category | flops | bytes accessed | tf_op | source)
XLA Modules:
  0.0 60.2 jit_solution(10044159621488295268)
XLA Ops:
  1.3 57.3 %layer.1 = (bf16[512,128]{1,0:T(8,128)(2,1)}, bf16[256,128]{1,0:T(8,128)(2,1)}) custom-call(bf16[512,128]{1,0:T(8,128)(2,1)} %bitcast.10, bf16[512,128]{1,0:T(8,128)(2,1)} %bitcast.11, bf16[512,128]{1,0:T(8,128)(2,1)} %bitcast.12, f32[1,1]{1,0:T(1,128)} %bitcast.9.mix_hbm, f32[1,128]{1,0:T(1,128)} %bitcast.16, bf16[256,128]{1,0:T(8,128)(2,1)} %tokens_hbm.1, ...), custom_call_target="tpu_custom_call" | custom-call | tf_op jit(solution)/shard_map/layer/pallas_call | solution.py:647
  58.6 1.6 %hand_on.1 = (bf16[512,128]{1,0:T(8,128)(2,1)}, bf16[256,128]{1,0:T(8,128)(2,1)}) custom-call(bf16[512,128]{1,0:T(8,128)(2,1)} %get-tuple-element.6.attn_in, bf16[256,128]{1,0:T(8,128)(2,1)} %get-tuple-element.7.moe_in), custom_call_target="tpu_custom_call" | custom-call | tf_op jit(solution)/shard_map/hand_on/pallas_call | solution.py:720

commit v6 on v5

--- a/solution.py
+++ b/solution.py
@@ -384,15 +384,23 @@
         return [functools.partial(work, 0), functools.partial(work, 1)]
 
     both_2 = jnp.logical_and(x_2, y_2)
+    mid = [
+        *pieces((y_1, ((-1, -1), (-1, 1)))),
+        *pieces((y_3, ((1, -1), (1, 1)))),
+        *pieces((both_2, ((0, 2), (2, 0))), (x_2, ((0, 2),)), (y_2, ((2, 0),))),
+    ]
+
+    def rest():
+        pass
+
     fillers = [
         *pieces((y_3, ((-1, 0), (1, 0))), (y_1, ((-1, 0),))),
         *pieces((x_3, ((0, -1), (0, 1))), (x_1, ((0, -1),))),
         lambda: spread(2),
-        *pieces((y_1, ((-1, -1), (-1, 1)))),
-        *pieces((y_3, ((1, -1), (1, 1)))),
-        *pieces((both_2, ((0, 2), (2, 0))), (x_2, ((0, 2),)), (y_2, ((2, 0),))),
-        lambda: None,
-        lambda: None,
+        rest,
+        *mid[:3],
+        rest,
+        *mid[3:],
         lambda: spread(3),
         *pieces((y_3, ((-1, 2), (1, 2))), (y_1, ((-1, 2),))),
         *pieces((y_2, ((2, -1), (2, 1)))),
@@ -534,7 +542,7 @@
                 e = 1 - way if step < 2 else way
                 pass_on(way, hop, step % 2 * 2 + e)
             if step == 2:
-                for g in {1: (), 2: (5, 6), 3: (7,)}[hop]:
+                for g in {1: (5, 6), 2: (7,), 3: ()}[hop]:
                     for h in range(2):
                         down(g, h)
 
@@ -546,7 +554,7 @@
         for e in range(2):
             he = 2 * h + e
             if he == 0:
-                fill(3)
+                fill(2)
             total = own_sum(last, he)
             for way in range(2):
                 total = arrived_sum(total, way, far - 1, he)
@@ -554,7 +562,7 @@
         back_send[h * half : (h + 1) * half] = (
             jnp.concatenate(totals, axis=1).reshape(half, 128).astype(BF16)
         )
-        for p in range(h * sources_half, (h + 1) * sources_half):
+        for p in reversed(range(h * sources_half, (h + 1) * sources_half)):
 
             @pl.when(px != p)
             def _(p=p):

time: 60.5 us -> 59.5 us (0.983)
  Pallas kernels: 58.9 us -> 58.1 us
    pallas_call x1, Pallas kernels: 57.3 us -> 56.5 us  [shards(): pl.pallas_call(functools.partial(kernel, cfg), name='layer', out_shape=(j...]
where the time goes in v6:
time: 59.5 us; the launch traced here: 59.4 us
  Pallas kernels  58.1 us (98%)
  between operations  1.29 us (2%)
    pallas_call x1, Pallas kernels, shards(): pl.pallas_call(functools.partial(kernel, cfg), name='layer', out_shape=(j...  56.5 us
    pallas_call x1, Pallas kernels, shards(): pl.pallas_call(hand_on, name='hand_on', out_shape=(jax.ShapeDtypeStruct(a...  1.59 us

profile of v6, /device:TPU:1, one launch (start us, length us, event | category | flops | bytes accessed | tf_op | source)
XLA Modules:
  0.0 59.4 jit_solution(15334996746517977347)
XLA Ops:
  1.3 56.5 %layer.1 = (bf16[512,128]{1,0:T(8,128)(2,1)}, bf16[256,128]{1,0:T(8,128)(2,1)}) custom-call(bf16[512,128]{1,0:T(8,128)(2,1)} %bitcast.10, bf16[512,128]{1,0:T(8,128)(2,1)} %bitcast.11, bf16[512,128]{1,0:T(8,128)(2,1)} %bitcast.12, f32[1,1]{1,0:T(1,128)} %bitcast.9.mix_hbm, f32[1,128]{1,0:T(1,128)} %bitcast.16, bf16[256,128]{1,0:T(8,128)(2,1)} %tokens_hbm.1, ...), custom_call_target="tpu_custom_call" | custom-call | tf_op jit(solution)/shard_map/layer/pallas_call | solution.py:655
  57.8 1.6 %hand_on.1 = (bf16[512,128]{1,0:T(8,128)(2,1)}, bf16[256,128]{1,0:T(8,128)(2,1)}) custom-call(bf16[512,128]{1,0:T(8,128)(2,1)} %get-tuple-element.6.attn_in, bf16[256,128]{1,0:T(8,128)(2,1)} %get-tuple-element.7.moe_in), custom_call_target="tpu_custom_call" | custom-call | tf_op jit(solution)/shard_map/hand_on/pallas_call | solution.py:728

commit v7 on v6

--- a/solution.py
+++ b/solution.py
@@ -68,8 +68,8 @@
     gate_hbm,
     up_hbm,
     down_hbm,
-    attn_hbm,
-    moe_hbm,
+    attn_ref,
+    moe_ref,
     q_ref,
     mix_ref,
     sub_gain_ref,
@@ -80,8 +80,6 @@
     gate_w,
     up_w,
     down_w,
-    attn_ref,
-    moe_ref,
     qz,
     kbuf,
     vbuf,
@@ -100,7 +98,6 @@
     back_send,
     back,
     in_sem,
-    out_sem,
     kv_send,
     kv_recv,
     d_send,
@@ -587,8 +584,6 @@
         mean = jnp.mean(blend * blend, axis=1, keepdims=True)
         scaled = blend * lax.rsqrt(mean + SUB_EPS)
         attn_ref[one, :] = (scaled * sub_gain_ref[...] * OUT_SCALE).astype(BF16)
-    attn_out = pltpu.make_async_copy(attn_ref, attn_hbm, out_sem.at[0])
-    attn_out.start()
 
     sent = outgoing.at[pl.ds(0, others)]
     remote(sent, sent, d_send.at[0], d_recv.at[0], ep, partner).wait_send()
@@ -612,15 +607,6 @@
     moe_ref[...] = (
         nn_dot(picks[0], result) * weight[:, 0:1] + nn_dot(picks[1], result) * weight[:, 1:2]
     ).astype(BF16)
-    moe_out = pltpu.make_async_copy(moe_ref, moe_hbm, out_sem.at[1])
-    moe_out.start()
-    attn_out.wait()
-    moe_out.wait()
-
-
-def hand_on(attn_in, moe_in, attn_ref, moe_ref):
-    attn_ref[...] = attn_in[...]
-    moe_ref[...] = moe_in[...]
 
 
 def shards(
@@ -652,15 +638,16 @@
     dma = pltpu.SemaphoreType.DMA
     vmem = pltpu.VMEM
     anywhere = pl.BlockSpec(memory_space=pl.ANY)
+    whole = pl.BlockSpec(memory_space=vmem)
     attn_out, moe_out = pl.pallas_call(
         functools.partial(kernel, cfg),
         name="layer",
         out_shape=(
-            jax.ShapeDtypeStruct((q_rows, v_width), BF16),
-            jax.ShapeDtypeStruct((rows, tokens.shape[1]), BF16),
+            vmem((q_rows, v_width), BF16),
+            vmem((rows, tokens.shape[1]), BF16),
         ),
         in_specs=[anywhere] * 12,
-        out_specs=(anywhere, anywhere),
+        out_specs=(whole, whole),
         scratch_shapes=[
             vmem((q_rows, qk_width), BF16),
             vmem((1, 1), F32),
@@ -672,8 +659,6 @@
             vmem(gate_weight.shape, BF16),
             vmem(up_weight.shape, BF16),
             vmem(down_weight.shape, BF16),
-            vmem((q_rows, v_width), BF16),
-            vmem((rows, tokens.shape[1]), BF16),
             vmem((2 * q_rows, qk_width), BF16),
             vmem((n_ep, q_rows, qk_width), BF16),
             vmem((n_ep, q_rows, v_width), BF16),
@@ -692,7 +677,6 @@
             vmem((slots, 128), BF16),
             vmem((slots, 128), BF16),
             dma((12,)),
-            dma((2,)),
             dma((2,)),
             dma((len(STAGES) - 1,)),
             dma((1,)),
@@ -724,17 +708,6 @@
         up_weight,
         down_weight,
     )
-    whole = pl.BlockSpec(memory_space=vmem)
-    attn_out, moe_out = pl.pallas_call(
-        hand_on,
-        name="hand_on",
-        out_shape=(
-            jax.ShapeDtypeStruct(attn_out.shape, BF16),
-            jax.ShapeDtypeStruct(moe_out.shape, BF16),
-        ),
-        in_specs=[whole] * 2,
-        out_specs=(whole, whole),
-    )(attn_out, moe_out)
     return attn_out.reshape(q_rows, 1, v_width), moe_out
 
 

time: 59.5 us -> 58.5 us (0.983)
  Pallas kernels: 58.1 us -> 55.9 us
  local copies, waits for them, and re-layouts: 0 us -> 1.29 us
    pallas_call x2 -> x1, Pallas kernels: 58.1 us -> 55.9 us  [shards(): pl.pallas_call(functools.partial(kernel, cfg), name='layer', out_shape=(v...]
    unnamed x0 -> x2, local copies, waits for them, and re-layouts: none -> 1.29 us
where the time goes in v7:
time: 58.5 us; the launch traced here: 58.4 us
  Pallas kernels  55.9 us (96%)
  local copies, waits for them, and re-layouts  1.29 us (2%)
  between operations  1.29 us (2%)
    pallas_call x1, Pallas kernels, shards(): pl.pallas_call(functools.partial(kernel, cfg), name='layer', out_shape=(v...  55.9 us
    unnamed x2, local copies, waits for them, and re-layouts  1.29 us

profile of v7, /device:TPU:1, one launch (start us, length us, event | category | flops | bytes accessed | tf_op | source)
XLA Modules:
  0.0 58.4 jit_solution(11130099738679575544)
XLA Ops:
  1.3 55.9 %layer.1 = (bf16[512,128]{1,0:T(8,128)(2,1)S(1)}, bf16[256,128]{1,0:T(8,128)(2,1)S(1)}) custom-call(bf16[512,128]{1,0:T(8,128)(2,1)} %bitcast.11, bf16[512,128]{1,0:T(8,128)(2,1)} %bitcast.12, bf16[512,128]{1,0:T(8,128)(2,1)} %bitcast.13, f32[1,1]{1,0:T(1,128)} %bitcast.9.mix_hbm, f32[1,128]{1,0:T(1,128)} %bitcast.17, bf16[256,128]{1,0:T(8,128)(2,1)} %tokens_hbm.1, ...), custom_call_target="tpu_custom_call" | custom-call | tf_op jit(solution)/shard_map/layer/pallas_call | solution.py:642
  57.2 0.7 %copy.16 = bf16[512,1,128]{2,0,1:T(8,128)(2,1)} copy(bf16[512,1,128]{2,0,1:T(8,128)(2,1)S(1)} %bitcast.10) | data formatting | bytes 262144
  57.8 0.6 %copy.17 = bf16[256,128]{1,0:T(8,128)(2,1)} copy(bf16[256,128]{1,0:T(8,128)(2,1)S(1)} %get-tuple-element.7) | data formatting | bytes 131072
